TPU v7x, 256 devices: a whole 4x4x8 slice. The times are simulated.
256 devices in a mesh: tp: 32 (over z, y), dp: 8 (over x, core).
Axes of the slice: x: 4, y: 4, z: 8, core: 2. Of those that a mesh axis runs over, the one named last changes fastest.
Arguments:
- stream: bfloat16 [256, 2048], P('tp', 'dp'), may hold values from -12 to 12
- norm_gain: float32 [2, 2048], P(None, 'dp'), may hold values from 0.1 to 1.9
- w_input: bfloat16 [2, 2048, 2048], P(None, 'dp', 'tp'), may hold values from -0.125 to 0.125
- lam_re: float32 [2, 128, 64], P(None, 'tp'), may hold values from -1 to -0.05
- lam_im: float32 [2, 128, 64], P(None, 'tp'), may hold values from 0 to 6
- log_dt: float32 [2, 128], P(None, 'tp'), may hold values from -3 to 0
- b_re: float32 [2, 128, 64, 16], P(None, 'tp'), may hold values from -1 to 1
- b_im: float32 [2, 128, 64, 16], P(None, 'tp'), may hold values from -1 to 1
- readout_real: float32 [2, 128, 16, 64], P(None, 'tp'), may hold values from -0.5 to 0.5
- readout_imaginary: float32 [2, 128, 16, 64], P(None, 'tp'), may hold values from -0.5 to 0.5
- d_skip: float32 [2, 2048], P(None, 'tp'), may hold values from -4 to 4
- w_val: bfloat16 [2, 2048, 2048], P(None, 'tp', 'dp'), may hold values from -0.375 to 0.375
- w_gate: bfloat16 [2, 2048, 2048], P(None, 'tp', 'dp'), may hold values from -0.375 to 0.375
- state: float32 [2, 256, 128, 128], P(None, 'dp', 'tp'), may hold values from -6 to 6
Outputs:
- stream_out: bfloat16 [256, 2048], P('tp', 'dp')
- states_out: float32 [2, 256, 128, 128], P(None, 'dp', 'tp')
All inputs are finite; a program needn't handle non-finite values.
Results may differ from a plain program's by a relative error of at most 0.0064.
Values may be sent and summed in bfloat16 or wider, within the bound.
A program may use at most 64 MiB of HBM per device.

v0:
```python
import functools

import jax
import jax.numpy as jnp
from jax import lax
from jax.experimental import pallas as pl
from jax.experimental.pallas import tpu as pltpu
from jax.sharding import PartitionSpec as P

EPS = 1e-06
F32 = jnp.float32
BF16 = jnp.bfloat16
HIGHEST = lax.Precision.HIGHEST
NT = (((1,), (1,)), ((), ()))


def partner(me, k, n, back=False):
    if n & (n - 1):
        return (me + (n - k if back else k)) % n
    found, bit = 0, 1
    while bit < n:
        mine = (me // bit) % 2
        found = found + (bit * (1 - mine) if k & bit else bit * mine)
        bit *= 2
    return found


def kernel(
    tp, dp, chans,
    stream_ref, gain_ref, w_in_hbm, lam_re_ref, lam_im_ref, log_dt_ref, b_re_hbm, b_im_hbm, c_re_hbm, c_im_hbm, skip_ref,
    w_val_hbm, w_gate_hbm, state_hbm,
    out_ref, state,
    w_in, w_val, w_gate, b_re, b_im, c_re, c_im, drive, read,
    kept, proj, u_keep, masked, from_old, mix_w,
    x_all, part_send, part_recv, sq_send, sq_recv, mix_all, comb_send, comb_own, comb_recv,
    load_sem, x_ss, x_rs, part_ss, part_rs, sq_ss, sq_rs, mix_ss, mix_rs, comb_ss, comb_rs,
):
    layers = w_in.shape[0]
    me_t, me_d = lax.axis_index("tp"), lax.axis_index("dp")
    rows_t, feats = stream_ref.shape
    rows_d, width = u_keep.shape[1:]
    per = rows_d // rows_t
    groups, half = lam_re_ref.shape[1:]
    lanes = state.shape[2]
    sq_width = sq_send.shape[3]

    loads = {}
    for l in range(layers):
        for i, (src, dst) in enumerate(
            (
                (b_re_hbm, b_re), (b_im_hbm, b_im), (c_re_hbm, c_re), (c_im_hbm, c_im), (state_hbm, state),
                (w_in_hbm, w_in), (w_val_hbm, w_val), (w_gate_hbm, w_gate),
            )
        ):
            loads[l, i] = pltpu.make_async_copy(src.at[l], dst.at[l], load_sem.at[l, i])
            loads[l, i].start()

    barrier = pltpu.get_barrier_semaphore()
    for k in range(1, dp):
        pl.semaphore_signal(barrier, inc=1, device_id={"dp": partner(me_d, k, dp)}, device_id_type=pl.DeviceIdType.MESH)
    for k in range(1, tp):
        pl.semaphore_signal(barrier, inc=1, device_id={"tp": partner(me_t, k, tp)}, device_id_type=pl.DeviceIdType.MESH)

    def send(src, dst, ss, rs, axis, to):
        return pltpu.make_async_remote_copy(
            src_ref=src, dst_ref=dst, send_sem=ss, recv_sem=rs, device_id={axis: to}, device_id_type=pl.DeviceIdType.MESH
        )

    def x_copy(l, k):
        src = stream_ref if l == 0 else x_all.at[l, me_t]
        to = partner(me_t, k, tp)
        return send(src, x_all.at[l, me_t], x_ss.at[l, to], x_rs.at[l, me_t], "tp", to)

    def part_copy(l, to):
        return send(part_send.at[l, to], part_recv.at[l, me_d], part_ss.at[l, to], part_rs.at[l, me_d], "dp", to)

    def sq_copy(l, to):
        return send(sq_send.at[l, to], sq_recv.at[l, me_d], sq_ss.at[l, to], sq_rs.at[l, me_d], "dp", to)

    def mix_copy(l, to):
        return send(mix_all.at[l, me_d], mix_all.at[l, me_d], mix_ss.at[l, to], mix_rs.at[l, me_d], "dp", to)

    def comb_copy(l, to):
        return send(comb_send.at[l, to], comb_recv.at[l, me_t], comb_ss.at[l, to], comb_rs.at[l, me_t], "tp", to)

    def arrival(ref, rs, axis):
        return send(ref, ref, rs, rs, axis, 0)

    lane_group = lax.broadcasted_iota(jnp.int32, (rows_d, width), 1) // chans
    eye = lax.broadcasted_iota(jnp.int32, (rows_d, sq_width), 0) == lax.broadcasted_iota(jnp.int32, (rows_d, sq_width), 1)

    group_eye = lax.broadcasted_iota(jnp.int32, (groups, groups), 0) == lax.broadcasted_iota(jnp.int32, (groups, groups), 1)

    def prepare(l):
        step_size = jnp.exp(jnp.sum(jnp.where(group_eye, log_dt_ref[l : l + 1, :], 0.0), axis=1, keepdims=True))
        lam_re, lam_im = lam_re_ref[l], lam_im_ref[l]
        decay = jnp.exp(lam_re * step_size)
        angle = lam_im * step_size
        keep_re = decay * jnp.cos(angle)
        keep_im = decay * jnp.sin(angle)
        denom = lam_re * lam_re + lam_im * lam_im
        ratio_re = ((keep_re - 1.0) * lam_re + keep_im * lam_im) / denom
        ratio_im = (keep_im * lam_re - (keep_re - 1.0) * lam_im) / denom
        keep_a = jnp.concatenate([keep_re, keep_re], axis=1)
        keep_b = jnp.concatenate([-keep_im, keep_im], axis=1)
        for i in range(5):
            loads[l, i].wait()
        for g in range(groups):
            t_re, t_im = b_re[l, g], b_im[l, g]
            r_re, r_im = ratio_re[g : g + 1, :], ratio_im[g : g + 1, :]
            drive[l, pl.ds(g * chans, chans), :] = jnp.concatenate(
                [r_re * t_re - r_im * t_im, r_re * t_im + r_im * t_re], axis=1
            )
        read[l] = jnp.concatenate([c_re[l].reshape(width, half), -c_im[l].reshape(width, half)], axis=1)
        for g in range(groups):
            old = state[l, pl.ds(g, rows_d, stride=groups), :]
            kept[l, pl.ds(g * rows_d, rows_d), :] = (
                keep_a[g : g + 1, :] * old + keep_b[g : g + 1, :] * pltpu.roll(old, lanes // 2, 1)
            )
        proj[...] = lax.dot_general(kept[l], read[l], NT, precision=HIGHEST, preferred_element_type=F32)
        total = jnp.zeros((rows_d, width), F32)
        for g in range(groups):
            total = jnp.where(lane_group == g, proj[pl.ds(g * rows_d, rows_d), :], total)
        from_old[l] = total
        full = lax.dot_general(drive[l], read[l], NT, precision=HIGHEST, preferred_element_type=F32)
        same = (
            lax.broadcasted_iota(jnp.int32, (width, width), 0) // chans
            == lax.broadcasted_iota(jnp.int32, (width, width), 1) // chans
        )
        mix_w[l] = jnp.where(same, full, 0.0)

    def update(l):
        u = u_keep[l]
        for g in range(groups):
            masked[pl.ds(g * rows_d, rows_d), :] = jnp.where(lane_group == g, u, 0.0)
        kept[l] = kept[l] + jnp.dot(masked[...], drive[l], precision=HIGHEST, preferred_element_type=F32)
        for g in range(groups):
            state[l, pl.ds(g, rows_d, stride=groups), :] = kept[l, pl.ds(g * rows_d, rows_d), :]

    pl.semaphore_wait(barrier, tp + dp - 2)
    for k in reversed(range(1, tp)):
        x_copy(0, k).start()
    x_all[0, me_t] = stream_ref[...]
    prepare(0)

    for l in range(layers):
        loads[l, 5].wait()
        gain = gain_ref[l : l + 1, :]
        own_part = own_sq = None
        for k in reversed(range(dp)):
            to = partner(me_d, k, dp)
            for j in range(per):
                t = to * per + j

                @pl.when(t != me_t)
                def _():
                    arrival(x_all.at[l, t], x_rs.at[l, t], "tp").wait_recv()

            x = x_all[l, pl.ds(to * per, per)].astype(F32).reshape(rows_d, feats)
            column = jnp.sum(x * x, axis=1, keepdims=True)
            squares = jnp.sum(jnp.where(eye, column, 0.0), axis=0, keepdims=True)
            product = jnp.dot((x * gain).astype(BF16), w_in[l], preferred_element_type=F32)
            if k:
                sq_send[l, to] = jnp.broadcast_to(squares, (8, sq_width))
                sq_copy(l, to).start()
                part_send[l, to] = product.astype(BF16)
                part_copy(l, to).start()
            else:
                own_part, own_sq = product, squares
        for k in range(1, dp):
            by = partner(me_d, k, dp, True)
            arrival(sq_recv.at[l, by], sq_rs.at[l, by], "dp").wait_recv()
            own_sq = own_sq + sq_recv[l, by][0:1, :]
            arrival(part_recv.at[l, by], part_rs.at[l, by], "dp").wait_recv()
            own_part = own_part + part_recv[l, by].astype(F32)
        square_total = jnp.sum(jnp.where(eye, own_sq, 0.0), axis=1, keepdims=True)
        u = lax.rsqrt(square_total / (feats * dp) + EPS) * own_part
        u_keep[l] = u
        pre = from_old[l] + jnp.dot(u, mix_w[l], precision=HIGHEST, preferred_element_type=F32) + skip_ref[l : l + 1, :] * u
        mix_all[l, me_d] = jax.nn.gelu(pre).astype(BF16)
        for k in reversed(range(1, dp)):
            mix_copy(l, partner(me_d, k, dp)).start()
        loads[l, 6].wait()
        loads[l, 7].wait()
        for k in range(dp):
            by = partner(me_d, k, dp, True)
            if k:
                arrival(mix_all.at[l, by], mix_rs.at[l, by], "dp").wait_recv()
            mixed = mix_all[l, by]
            value = jnp.dot(mixed, w_val[l], preferred_element_type=F32)
            gate = jnp.dot(mixed, w_gate[l], preferred_element_type=F32)
            for j in range(per):
                t = by * per + j
                rows = slice(j * rows_t, (j + 1) * rows_t)

                @pl.when(t != me_t)
                def _():
                    comb_send[l, t, :, :feats] = value[rows].astype(BF16)
                    comb_send[l, t, :, feats:] = gate[rows].astype(BF16)
                    comb_copy(l, t).start()

                @pl.when(t == me_t)
                def _():
                    comb_own[:, :feats] = value[rows]
                    comb_own[:, feats:] = gate[rows]

        update(l)
        if l + 1 < layers:
            prepare(l + 1)
        combined = comb_own[...]
        for k in range(1, tp):
            by = partner(me_t, k, tp, True)
            arrival(comb_recv.at[l, by], comb_rs.at[l, by], "tp").wait_recv()
            combined = combined + comb_recv[l, by].astype(F32)
        fresh = (
            x_all[l, me_t].astype(F32) + combined[:, :feats] * jax.nn.sigmoid(combined[:, feats:])
        ).astype(BF16)
        if l + 1 < layers:
            x_all[l + 1, me_t] = fresh
            for k in reversed(range(1, tp)):
                x_copy(l + 1, k).start()
        else:
            out_ref[...] = fresh

    for l in range(layers):
        for k in range(1, tp):
            x_copy(l, k).wait_send()
            comb_copy(l, partner(me_t, k, tp)).wait_send()
        for k in range(1, dp):
            to = partner(me_d, k, dp)
            part_copy(l, to).wait_send()
            sq_copy(l, to).wait_send()
            mix_copy(l, to).wait_send()


def per_device(
    tp, dp,
    stream, norm_gain, w_input, lam_re, lam_im, log_dt, b_re, b_im, readout_real, readout_imaginary, d_skip,
    w_val, w_gate, state,
):
    layers, feats, width = w_input.shape
    rows_t = stream.shape[0]
    rows_d, groups, lanes = state.shape[1:]
    chans = b_re.shape[-1]

    turned_re, turned_im = b_re.swapaxes(2, 3), b_im.swapaxes(2, 3)

    limit = 67043328 - 4 * layers * rows_d * groups * lanes - (256 << 10)
    vmem = pl.BlockSpec(memory_space=pltpu.VMEM)
    hbm = pl.BlockSpec(memory_space=pltpu.HBM)
    sq_width = max(rows_d, 128)
    dma = lambda *shape: pltpu.SemaphoreType.DMA(shape)
    out, states = pl.pallas_call(
        functools.partial(kernel, tp, dp, chans),
        out_shape=(pltpu.VMEM(stream.shape, BF16), pltpu.VMEM((layers, rows_d * groups, lanes), F32)),
        in_specs=[vmem, vmem, hbm, vmem, vmem, vmem, hbm, hbm, hbm, hbm, vmem, hbm, hbm, hbm],
        out_specs=(vmem, vmem),
        scratch_shapes=[
            pltpu.VMEM(w_input.shape, BF16),
            pltpu.VMEM(w_val.shape, BF16),
            pltpu.VMEM(w_gate.shape, BF16),
            pltpu.VMEM(turned_re.shape, F32),
            pltpu.VMEM(turned_im.shape, F32),
            pltpu.VMEM(readout_real.shape, F32),
            pltpu.VMEM(readout_imaginary.shape, F32),
            pltpu.VMEM((layers, width, lanes), F32),
            pltpu.VMEM((layers, width, lanes), F32),
            pltpu.VMEM((layers, rows_d * groups, lanes), F32),
            pltpu.VMEM((rows_d * groups, width), F32),
            pltpu.VMEM((layers, rows_d, width), F32),
            pltpu.VMEM((rows_d * groups, width), F32),
            pltpu.VMEM((layers, rows_d, width), F32),
            pltpu.VMEM((layers, width, width), F32),
            pltpu.VMEM((layers, tp, rows_t, feats), BF16),
            pltpu.VMEM((layers, dp, rows_d, width), BF16),
            pltpu.VMEM((layers, dp, rows_d, width), BF16),
            pltpu.VMEM((layers, dp, 8, sq_width), F32),
            pltpu.VMEM((layers, dp, 8, sq_width), F32),
            pltpu.VMEM((layers, dp, rows_d, width), BF16),
            pltpu.VMEM((layers, tp, rows_t, 2 * feats), BF16),
            pltpu.VMEM((rows_t, 2 * feats), F32),
            pltpu.VMEM((layers, tp, rows_t, 2 * feats), BF16),
            dma(layers, 8),
            dma(layers, tp), dma(layers, tp),
            dma(layers, dp), dma(layers, dp),
            dma(layers, dp), dma(layers, dp),
            dma(layers, dp), dma(layers, dp),
            dma(layers, tp), dma(layers, tp),
        ],
        compiler_params=pltpu.CompilerParams(collective_id=0, has_side_effects=True, vmem_limit_bytes=limit),
    )(
        stream, norm_gain, w_input, lam_re, lam_im, log_dt, turned_re, turned_im, readout_real,
        readout_imaginary, d_skip, w_val, w_gate,
        state.reshape(layers, rows_d * groups, lanes),
    )
    return out, states.reshape(state.shape)


def solution(mesh):
    return jax.shard_map(
        functools.partial(per_device, mesh.shape["tp"], mesh.shape["dp"]),
        mesh=mesh,
        in_specs=(
            P("tp", "dp"),
            P(None, "dp"),
            P(None, "dp", "tp"),
            P(None, "tp", None),
            P(None, "tp", None),
            P(None, "tp"),
            P(None, "tp", None, None),
            P(None, "tp", None, None),
            P(None, "tp", None, None),
            P(None, "tp", None, None),
            P(None, "tp"),
            P(None, "tp", "dp"),
            P(None, "tp", "dp"),
            P(None, "dp", "tp", None),
        ),
        out_specs=(P("tp", "dp"), P(None, "dp", "tp", None)),
        check_vma=False,
    )
```

profile of v0, /device:TPU:39, one launch (start us, length us, event | category | flops | bytes accessed | tf_op | source)
XLA Modules:
  0.0 65.1 jit_solution(14453179211707751361)
XLA Ops:
  0.6 1.6 %copy.16.w_in_hbm = bf16[2,256,64]{2,1,0:T(8,128)(2,1)} copy(bf16[2,256,64]{1,2,0:T(8,128)(2,1)} %param.16) | data formatting | bytes 131072 | tf_op args[2]
  2.2 61.6 %shard_map.149 = (bf16[8,256]{1,0:T(8,128)(2,1)S(1)}, f32[2,128,128]{2,1,0:T(8,128)S(1)}) custom-call(bf16[8,256]{1,0:T(8,128)(2,1)} %stream_ref.1, f32[2,256]{1,0:T(2,128)} %gain_ref.1, bf16[2,256,64]{2,1,0:T(8,128)(2,1)} %copy.16.w_in_hbm, f32[2,4,64]{2,1,0:T(4,128)} %lam_re_ref.1, f32[2,4,64]{2,1,0:T(4,128)} %lam_im_ref.1, f32[2,4]{1,0:T(2,128)} %log_dt_ref.1, ...), custom_call_target="tpu_custom_call" | custom-call | tf_op jit(solution)/shard_map/pallas_call | solution.py:253
  63.8 0.6 copy.19
  64.4 0.7 %copy.20 = f32[2,32,4,128]{3,2,1,0:T(4,128)} copy(f32[2,32,4,128]{3,2,1,0:T(4,128)S(1)} %bitcast.4) | data formatting | bytes 262144
where the time goes:
time: 65.2 us; the launch traced here: 65.1 us
  Pallas kernels  61.6 us (94%)
  local copies, waits for them, and re-layouts  2.85 us (4%)
    pallas_call x1, Pallas kernels, per_device(): pl.pallas_call(functools.partial(kernel, tp, dp, chans), out_shape=(pltpu...  61.6 us
    unnamed x3, local copies, waits for them, and re-layouts  2.85 us

commit v1 on v0

v1 whole, which is shorter than its diff:
```python
import functools

import jax
import jax.numpy as jnp
from jax import lax
from jax.experimental import pallas as pl
from jax.experimental.pallas import tpu as pltpu
from jax.sharding import PartitionSpec as P

EPS = 1e-06
F32 = jnp.float32
BF16 = jnp.bfloat16
HIGHEST = lax.Precision.HIGHEST
NT = (((1,), (1,)), ((), ()))
PLANE_FAR_FIRST = (4, 5, 6, 7, 2, 3, 1, 0)
ROW_FAR_FIRST = (2, 1, 3, 0)


def partner(me, k, n, back=False):
    if n & (n - 1):
        return (me + (n - k if back else k)) % n
    found, bit = 0, 1
    while bit < n:
        mine = (me // bit) % 2
        found = found + (bit * (1 - mine) if k & bit else bit * mine)
        bit *= 2
    return found


def kernel(
    tp, dp, chans,
    stream_ref, gain_ref, w_in_hbm, lam_re_ref, lam_im_ref, log_dt_ref, b_re_hbm, b_im_hbm, c_re_hbm, c_im_hbm, skip_ref,
    w_val_hbm, w_gate_hbm, state_hbm,
    out_ref, state,
    w_in, w_val, w_gate, b_re, b_im, c_re, c_im, drive, read,
    kept, proj, u_keep, masked, from_old, mix_w,
    x_all, part_send, part_recv, sq_send, sq_recv, mix_all, comb_send, comb_own, comb_recv,
    gain_all, far_in, far_val, far_gate, x_far, swap_send, swap_recv, u_send, u_recv, out_send, out_recv,
    load_sem, x_ss, x_rs, part_ss, part_rs, sq_ss, sq_rs, mix_ss, mix_rs, comb_ss, comb_rs,
    gain_ss, gain_rs, far_ss, far_rs, xf_ss, xf_rs, swap_ss, swap_rs, u_ss, u_rs, of_ss, of_rs,
):
    layers = w_in.shape[0]
    me_t, me_d = lax.axis_index("tp"), lax.axis_index("dp")
    rows_t, feats = stream_ref.shape
    rows_d, width = u_keep.shape
    per = rows_d // rows_t
    groups, half = lam_re_ref.shape[1:]
    lanes = state.shape[2]
    sq_width = sq_send.shape[2]
    me_z, me_y = me_t // per, me_t % per

    loads = {}
    for l in range(layers):
        for i, (src, dst) in enumerate(
            (
                (b_re_hbm, b_re), (b_im_hbm, b_im), (c_re_hbm, c_re), (c_im_hbm, c_im), (state_hbm, state),
                (w_in_hbm, w_in), (w_val_hbm, w_val), (w_gate_hbm, w_gate),
            )
        ):
            loads[l, i] = pltpu.make_async_copy(src.at[l], dst.at[l], load_sem.at[l, i])
            loads[l, i].start()

    barrier = pltpu.get_barrier_semaphore()

    def greet(t, d):
        pl.semaphore_signal(barrier, inc=1, device_id={"tp": t, "dp": d}, device_id_type=pl.DeviceIdType.MESH)

    for k in range(1, dp):
        greet(me_t, partner(me_d, k, dp))
    for k in range(1, tp):
        greet(partner(me_t, k, tp), me_d)
    for j in range(1, per):
        for k in range(1, dp):
            greet(me_z * per + partner(me_y, j, per), partner(me_d, k, dp))
    for k in range(dp):

        @pl.when(jnp.logical_or(me_z != me_d, k != me_d))
        def _():
            greet(me_d * per + me_y, k)

    def send(src, dst, ss, rs, t, d):
        return pltpu.make_async_remote_copy(
            src_ref=src, dst_ref=dst, send_sem=ss, recv_sem=rs, device_id={"tp": t, "dp": d},
            device_id_type=pl.DeviceIdType.MESH,
        )

    def x_copy(k):
        to = partner(me_t, k, tp)
        return send(stream_ref, x_all.at[me_t], x_ss.at[to], x_rs.at[me_t], to, me_d)

    def part_copy(to):
        return send(part_send.at[to], part_recv.at[me_d], part_ss.at[to], part_rs.at[me_d], me_t, to)

    def sq_copy(to):
        return send(sq_send.at[to], sq_recv.at[me_d], sq_ss.at[to], sq_rs.at[me_d], me_t, to)

    def mix_copy(to):
        return send(mix_all.at[me_d], mix_all.at[me_d], mix_ss.at[to], mix_rs.at[me_d], me_t, to)

    def comb_copy(to):
        return send(comb_send.at[to], comb_recv.at[me_t], comb_ss.at[to], comb_rs.at[me_t], to, me_d)

    def gain_copy(to):
        return send(gain_all.at[me_d], gain_all.at[me_d], gain_ss.at[to], gain_rs.at[me_d], me_t, to)

    far = ((w_in, far_in), (w_val, far_val), (w_gate, far_gate))

    def far_copy(i, z):
        return send(far[i][0].at[1], far[i][1].at[me_d], far_ss.at[i, z], far_rs.at[i, me_d], z * per + me_y, me_z)

    def xf_copy(y, d):
        return send(x_far.at[me_d, me_y], x_far.at[me_d, me_y], xf_ss.at[d, y], xf_rs.at[me_d, me_y], me_z * per + y, d)

    def of_copy(y, d):
        return send(out_send.at[d, y], out_recv.at[me_d, me_y], of_ss.at[d, y], of_rs.at[me_d, me_y], me_z * per + y, d)

    def swap_copy():
        return send(swap_send, swap_recv, swap_ss, swap_rs, me_d * per + me_y, me_z)

    def u_copy():
        return send(u_send, u_recv, u_ss, u_rs, me_d * per + me_y, me_z)

    def arrival(ref, rs):
        return send(ref, ref, rs, rs, 0, 0)

    def spread(i):
        loads[1, 5 + i].wait()
        for k in reversed(range(dp)):
            z = partner(me_z, k, dp)

            @pl.when(jnp.logical_or(z != me_z, me_z != me_d))
            def _():
                far_copy(i, z).start()

        @pl.when(me_z == me_d)
        def _():
            far[i][1][me_d] = far[i][0][1]

    def spread_wait(i, d):
        @pl.when(jnp.logical_or(d != me_d, me_z != me_d))
        def _():
            arrival(far[i][1].at[d], far_rs.at[i, d]).wait_recv()

    lane_group = lax.broadcasted_iota(jnp.int32, (rows_d, width), 1) // chans
    eye = lax.broadcasted_iota(jnp.int32, (rows_d, sq_width), 0) == lax.broadcasted_iota(jnp.int32, (rows_d, sq_width), 1)
    group_eye = lax.broadcasted_iota(jnp.int32, (groups, groups), 0) == lax.broadcasted_iota(jnp.int32, (groups, groups), 1)
    wide_0 = lax.broadcasted_iota(jnp.int32, (width, width), 0)
    wide_1 = lax.broadcasted_iota(jnp.int32, (width, width), 1)

    def prepare(l):
        step_size = jnp.exp(jnp.sum(jnp.where(group_eye, log_dt_ref[l : l + 1, :], 0.0), axis=1, keepdims=True))
        lam_re, lam_im = lam_re_ref[l], lam_im_ref[l]
        decay = jnp.exp(lam_re * step_size)
        angle = lam_im * step_size
        keep_re = decay * jnp.cos(angle)
        keep_im = decay * jnp.sin(angle)
        denom = lam_re * lam_re + lam_im * lam_im
        ratio_re = ((keep_re - 1.0) * lam_re + keep_im * lam_im) / denom
        ratio_im = (keep_im * lam_re - (keep_re - 1.0) * lam_im) / denom
        keep_a = jnp.concatenate([keep_re, keep_re], axis=1)
        keep_b = jnp.concatenate([-keep_im, keep_im], axis=1)
        for i in range(5):
            loads[l, i].wait()
        for g in range(groups):
            t_re, t_im = b_re[l, g], b_im[l, g]
            r_re, r_im = ratio_re[g : g + 1, :], ratio_im[g : g + 1, :]
            drive[l, pl.ds(g * chans, chans), :] = jnp.concatenate(
                [r_re * t_re - r_im * t_im, r_re * t_im + r_im * t_re], axis=1
            )
        read[l] = jnp.concatenate([c_re[l].reshape(width, half), -c_im[l].reshape(width, half)], axis=1)
        for g in range(groups):
            old = state[l, pl.ds(g, rows_d, stride=groups), :]
            kept[l, pl.ds(g * rows_d, rows_d), :] = (
                keep_a[g : g + 1, :] * old + keep_b[g : g + 1, :] * pltpu.roll(old, lanes // 2, 1)
            )
        proj[...] = lax.dot_general(kept[l], read[l], NT, precision=HIGHEST, preferred_element_type=F32)
        total = jnp.zeros((rows_d, width), F32)
        for g in range(groups):
            total = jnp.where(lane_group == g, proj[pl.ds(g * rows_d, rows_d), :], total)
        full = lax.dot_general(drive[l], read[l], NT, precision=HIGHEST, preferred_element_type=F32)
        mixer = jnp.where(wide_0 // chans == wide_1 // chans, full, 0.0)
        mixer = mixer + jnp.where(wide_0 == wide_1, skip_ref[l : l + 1, :], 0.0)
        return total, mixer

    def update(l, u):
        for g in range(groups):
            masked[pl.ds(g * rows_d, rows_d), :] = jnp.where(lane_group == g, u, 0.0)
        kept[l] = kept[l] + jnp.dot(masked[...], drive[l], precision=HIGHEST, preferred_element_type=F32)
        for g in range(groups):
            state[l, pl.ds(g, rows_d, stride=groups), :] = kept[l, pl.ds(g * rows_d, rows_d), :]

    elsewhere = ((me_z - me_d) * (me_z - me_d) + dp * dp - 1) // (dp * dp)
    pl.semaphore_wait(barrier, tp - 1 + dp - 1 + (per - 1) * (dp - 1) + dp - 1 + elsewhere)

    for k in reversed(range(1, tp)):
        x_copy(k).start()
    gain_all[me_d] = jnp.broadcast_to(gain_ref[1:2, :], (rows_t, feats))
    for k in reversed(range(1, dp)):
        gain_copy(partner(me_d, k, dp)).start()
    spread(0)
    x_all[me_t] = stream_ref[...]
    from_old[...], mix_w[...] = prepare(0)

    loads[0, 5].wait()
    gain = gain_ref[0:1, :]
    own_part = own_sq = None
    for k in reversed(range(dp)):
        to = partner(me_d, k, dp)
        for j in range(per):
            t = to * per + j

            @pl.when(t != me_t)
            def _():
                arrival(x_all.at[t], x_rs.at[t]).wait_recv()

        x = x_all[pl.ds(to * per, per)].astype(F32).reshape(rows_d, feats)
        column = jnp.sum(x * x, axis=1, keepdims=True)
        squares = jnp.sum(jnp.where(eye, column, 0.0), axis=0, keepdims=True)
        product = lax.dot_general((x * gain).astype(BF16), w_in[0], NT, preferred_element_type=F32)
        if k:
            sq_send[to] = jnp.broadcast_to(squares, (8, sq_width))
            sq_copy(to).start()
            part_send[to] = product.astype(BF16)
            part_copy(to).start()
        else:
            own_part, own_sq = product, squares
    spread(1)
    for k in range(1, dp):
        by = partner(me_d, k, dp, True)
        arrival(sq_recv.at[by], sq_rs.at[by]).wait_recv()
        own_sq = own_sq + sq_recv[by][0:1, :]
        arrival(part_recv.at[by], part_rs.at[by]).wait_recv()
        own_part = own_part + part_recv[by].astype(F32)
    square_total = jnp.sum(jnp.where(eye, own_sq, 0.0), axis=1, keepdims=True)
    u = lax.rsqrt(square_total / (feats * dp) + EPS) * own_part
    u_keep[...] = u
    pre = from_old[...] + jnp.dot(u, mix_w[...], precision=HIGHEST, preferred_element_type=F32)
    mix_all[me_d] = jax.nn.gelu(pre).astype(BF16)
    for k in reversed(range(1, dp)):
        mix_copy(partner(me_d, k, dp)).start()
    loads[0, 6].wait()
    loads[0, 7].wait()
    for k in range(dp):
        by = partner(me_d, k, dp, True)
        if k:
            arrival(mix_all.at[by], mix_rs.at[by]).wait_recv()
        mixed = mix_all[by]
        value = jnp.dot(mixed, w_val[0], preferred_element_type=F32)
        gate = jnp.dot(mixed, w_gate[0], preferred_element_type=F32)
        for j in range(per):
            t = by * per + j
            rows = slice(j * rows_t, (j + 1) * rows_t)

            @pl.when(t != me_t)
            def _():
                comb_send[t, :, :feats] = value[rows].astype(BF16)
                comb_send[t, :, feats:] = gate[rows].astype(BF16)
                comb_copy(t).start()

            @pl.when(t == me_t)
            def _():
                comb_own[:, :feats] = value[rows]
                comb_own[:, feats:] = gate[rows]

    spread(2)
    update(0, u_keep[...])
    total, mixer = prepare(1)
    swap_send[:rows_d] = jnp.concatenate([total, total], axis=1)
    swap_send[rows_d:] = jnp.concatenate([mixer, mixer], axis=1)

    @pl.when(me_z != me_d)
    def _():
        swap_copy().start()

    @pl.when(me_z == me_d)
    def _():
        swap_recv[...] = swap_send[...]

    combined = comb_own[...]
    for k in range(1, tp):
        by = partner(me_t, k, tp, True)
        arrival(comb_recv.at[by], comb_rs.at[by]).wait_recv()
        combined = combined + comb_recv[by].astype(F32)
    fresh = (x_all[me_t].astype(F32) + combined[:, :feats] * jax.nn.sigmoid(combined[:, feats:])).astype(BF16)

    x_far[me_d, me_y] = fresh
    for k in PLANE_FAR_FIRST:
        for j in ROW_FAR_FIRST:
            if k or j:
                xf_copy(partner(me_y, j, per), partner(me_d, k, dp)).start()
    for k in range(1, dp):
        by = partner(me_d, k, dp, True)
        arrival(gain_all.at[by], gain_rs.at[by]).wait_recv()

    acc = jnp.zeros((rows_d, width), F32)
    squares = jnp.zeros((rows_d, feats), F32)
    for k in reversed(PLANE_FAR_FIRST):
        by = partner(me_d, k, dp, True)
        spread_wait(0, by)
        for j in reversed(ROW_FAR_FIRST):
            if k or j:
                y = partner(me_y, j, per)
                arrival(x_far.at[by, y], xf_rs.at[by, y]).wait_recv()
        x = x_far[by].astype(F32)
        normed = (x * gain_all[by][None]).astype(BF16).reshape(rows_d, feats)
        x = x.reshape(rows_d, feats)
        squares = squares + x * x
        acc = acc + lax.dot_general(normed, far_in[by], NT, preferred_element_type=F32)
    u = lax.rsqrt(jnp.sum(squares, axis=1, keepdims=True) / (feats * dp) + EPS) * acc
    u_send[...] = jnp.concatenate([u, u], axis=1)

    @pl.when(me_z != me_d)
    def _():
        u_copy().start()
        arrival(swap_recv, swap_rs).wait_recv()

    @pl.when(me_z == me_d)
    def _():
        u_recv[...] = u_send[...]

    pre = swap_recv[:rows_d, :width] + jnp.dot(
        u, swap_recv[rows_d:, :width], precision=HIGHEST, preferred_element_type=F32
    )
    mixed = jax.nn.gelu(pre).astype(BF16)
    for k in PLANE_FAR_FIRST:
        to = partner(me_d, k, dp)
        spread_wait(1, to)
        spread_wait(2, to)
        value = jnp.dot(mixed, far_val[to], preferred_element_type=F32)
        gate = jnp.dot(mixed, far_gate[to], preferred_element_type=F32)
        out_send[to, :, :, :feats] = value.astype(BF16).reshape(per, rows_t, feats)
        out_send[to, :, :, feats:] = gate.astype(BF16).reshape(per, rows_t, feats)
        for j in ROW_FAR_FIRST:
            if k or j:
                of_copy(partner(me_y, j, per), to).start()
    combined = out_send[me_d, me_y].astype(F32)

    @pl.when(me_z != me_d)
    def _():
        arrival(u_recv, u_rs).wait_recv()

    update(1, u_recv[:, :width])
    for k in reversed(PLANE_FAR_FIRST):
        by = partner(me_d, k, dp, True)
        for j in reversed(ROW_FAR_FIRST):
            if k or j:
                y = partner(me_y, j, per)
                arrival(out_recv.at[by, y], of_rs.at[by, y]).wait_recv()
                combined = combined + out_recv[by, y].astype(F32)
    out_ref[...] = (
        x_far[me_d, me_y].astype(F32) + combined[:, :feats] * jax.nn.sigmoid(combined[:, feats:])
    ).astype(BF16)

    for k in range(1, tp):
        x_copy(k).wait_send()
        comb_copy(partner(me_t, k, tp)).wait_send()
    for k in range(1, dp):
        to = partner(me_d, k, dp)
        part_copy(to).wait_send()
        sq_copy(to).wait_send()
        mix_copy(to).wait_send()
        gain_copy(to).wait_send()
    for k in range(dp):
        z = partner(me_z, k, dp)

        @pl.when(jnp.logical_or(z != me_z, me_z != me_d))
        def _():
            for i in range(3):
                far_copy(i, z).wait_send()

    for k in range(dp):
        for j in range(per):
            if k or j:
                xf_copy(partner(me_y, j, per), partner(me_d, k, dp)).wait_send()
                of_copy(partner(me_y, j, per), partner(me_d, k, dp)).wait_send()

    @pl.when(me_z != me_d)
    def _():
        swap_copy().wait_send()
        u_copy().wait_send()


def per_device(
    tp, dp,
    stream, norm_gain, w_input, lam_re, lam_im, log_dt, b_re, b_im, readout_real, readout_imaginary, d_skip,
    w_val, w_gate, state,
):
    layers, feats, width = w_input.shape
    rows_t = stream.shape[0]
    rows_d, groups, lanes = state.shape[1:]
    chans = b_re.shape[-1]
    per = rows_d // rows_t

    turned_in = w_input.swapaxes(1, 2)
    turned_re, turned_im = b_re.swapaxes(2, 3), b_im.swapaxes(2, 3)

    limit = 67043328 - 4 * layers * rows_d * groups * lanes - (256 << 10)
    vmem = pl.BlockSpec(memory_space=pltpu.VMEM)
    hbm = pl.BlockSpec(memory_space=pltpu.HBM)
    sq_width = max(rows_d, 128)
    dma = lambda *shape: pltpu.SemaphoreType.DMA(shape)
    out, states = pl.pallas_call(
        functools.partial(kernel, tp, dp, chans),
        out_shape=(pltpu.VMEM(stream.shape, BF16), pltpu.VMEM((layers, rows_d * groups, lanes), F32)),
        in_specs=[vmem, vmem, hbm, vmem, vmem, vmem, hbm, hbm, hbm, hbm, vmem, hbm, hbm, hbm],
        out_specs=(vmem, vmem),
        scratch_shapes=[
            pltpu.VMEM(turned_in.shape, BF16),
            pltpu.VMEM(w_val.shape, BF16),
            pltpu.VMEM(w_gate.shape, BF16),
            pltpu.VMEM(turned_re.shape, F32),
            pltpu.VMEM(turned_im.shape, F32),
            pltpu.VMEM(readout_real.shape, F32),
            pltpu.VMEM(readout_imaginary.shape, F32),
            pltpu.VMEM((layers, width, lanes), F32),
            pltpu.VMEM((layers, width, lanes), F32),
            pltpu.VMEM((layers, rows_d * groups, lanes), F32),
            pltpu.VMEM((rows_d * groups, width), F32),
            pltpu.VMEM((rows_d, width), F32),
            pltpu.VMEM((rows_d * groups, width), F32),
            pltpu.VMEM((rows_d, width), F32),
            pltpu.VMEM((width, width), F32),
            pltpu.VMEM((tp, rows_t, feats), BF16),
            pltpu.VMEM((dp, rows_d, width), BF16),
            pltpu.VMEM((dp, rows_d, width), BF16),
            pltpu.VMEM((dp, 8, sq_width), F32),
            pltpu.VMEM((dp, 8, sq_width), F32),
            pltpu.VMEM((dp, rows_d, width), BF16),
            pltpu.VMEM((tp, rows_t, 2 * feats), BF16),
            pltpu.VMEM((rows_t, 2 * feats), F32),
            pltpu.VMEM((tp, rows_t, 2 * feats), BF16),
            pltpu.VMEM((dp, rows_t, feats), F32),
            pltpu.VMEM((dp, width, feats), BF16),
            pltpu.VMEM((dp, width, feats), BF16),
            pltpu.VMEM((dp, width, feats), BF16),
            pltpu.VMEM((dp, per, rows_t, feats), BF16),
            pltpu.VMEM((rows_d + width, 128), F32),
            pltpu.VMEM((rows_d + width, 128), F32),
            pltpu.VMEM((rows_d, 128), F32),
            pltpu.VMEM((rows_d, 128), F32),
            pltpu.VMEM((dp, per, rows_t, 2 * feats), BF16),
            pltpu.VMEM((dp, per, rows_t, 2 * feats), BF16),
            dma(layers, 8),
            dma(tp), dma(tp),
            dma(dp), dma(dp),
            dma(dp), dma(dp),
            dma(dp), dma(dp),
            dma(tp), dma(tp),
            dma(dp), dma(dp),
            dma(3, dp), dma(3, dp),
            dma(dp, per), dma(dp, per),
            pltpu.SemaphoreType.DMA, pltpu.SemaphoreType.DMA,
            pltpu.SemaphoreType.DMA, pltpu.SemaphoreType.DMA,
            dma(dp, per), dma(dp, per),
        ],
        compiler_params=pltpu.CompilerParams(collective_id=0, has_side_effects=True, vmem_limit_bytes=limit),
    )(
        stream, norm_gain, turned_in, lam_re, lam_im, log_dt, turned_re, turned_im, readout_real,
        readout_imaginary, d_skip, w_val, w_gate,
        state.reshape(layers, rows_d * groups, lanes),
    )
    return out, states.reshape(state.shape)


def solution(mesh):
    return jax.shard_map(
        functools.partial(per_device, mesh.shape["tp"], mesh.shape["dp"]),
        mesh=mesh,
        in_specs=(
            P("tp", "dp"),
            P(None, "dp"),
            P(None, "dp", "tp"),
            P(None, "tp", None),
            P(None, "tp", None),
            P(None, "tp"),
            P(None, "tp", None, None),
            P(None, "tp", None, None),
            P(None, "tp", None, None),
            P(None, "tp", None, None),
            P(None, "tp"),
            P(None, "tp", "dp"),
            P(None, "tp", "dp"),
            P(None, "dp", "tp", None),
        ),
        out_specs=(P("tp", "dp"), P(None, "dp", "tp", None)),
        check_vma=False,
    )
```

time: 65.2 us -> 57 us (0.87)
  the two profiles are of different devices: /device:TPU:39 before, /device:TPU:1 now
where the time goes in v1:
time: 57 us; the launch traced here: 56.9 us
  Pallas kernels  55 us (96%)
  local copies, waits for them, and re-layouts  1.25 us (2%)
  between operations  0.64 us (1%)
    pallas_call x1, Pallas kernels, per_device(): pl.pallas_call(functools.partial(kernel, tp, dp, chans), out_shape=(pltpu...  55 us
    unnamed x2, local copies, waits for them, and re-layouts  1.25 us

profile of v1, /device:TPU:1, one launch (start us, length us, event | category | flops | bytes accessed | tf_op | source)
XLA Modules:
  0.0 56.9 jit_solution(1531066447161622181)
XLA Ops:
  0.6 55.0 %shard_map.149 = (bf16[8,256]{1,0:T(8,128)(2,1)S(1)}, f32[2,128,128]{2,1,0:T(8,128)S(1)}) custom-call(bf16[8,256]{1,0:T(8,128)(2,1)} %stream_ref.1, f32[2,256]{1,0:T(2,128)} %gain_ref.1, bf16[2,64,256]{2,1,0:T(8,128)(2,1)} %bitcast.7, f32[2,4,64]{2,1,0:T(4,128)} %lam_re_ref.1, f32[2,4,64]{2,1,0:T(4,128)} %lam_im_ref.1, f32[2,4]{1,0:T(2,128)} %log_dt_ref.1, ...), custom_call_target="tpu_custom_call" | custom-call | tf_op jit(solution)/shard_map/pallas_call | solution.py:402
  55.6 0.6 %copy.18 = bf16[8,256]{1,0:T(8,128)(2,1)} copy(bf16[8,256]{1,0:T(8,128)(2,1)S(1)} %get-tuple-element.6) | data formatting | bytes 8192
  56.2 0.7 %copy.19 = f32[2,32,4,128]{3,2,1,0:T(4,128)} copy(f32[2,32,4,128]{3,2,1,0:T(4,128)S(1)} %bitcast.5) | data formatting | bytes 262144

commit v2 on v1

--- a/solution.py
+++ b/solution.py
@@ -29,17 +29,17 @@
 
 def kernel(
     tp, dp, chans,
-    stream_ref, gain_ref, w_in_hbm, lam_re_ref, lam_im_ref, log_dt_ref, b_re_hbm, b_im_hbm, c_re_hbm, c_im_hbm, skip_ref,
+    stream_hbm, gain_hbm, w_in_hbm, lam_re_hbm, lam_im_hbm, log_dt_hbm, b_re_hbm, b_im_hbm, c_re_hbm, c_im_hbm, skip_hbm,
     w_val_hbm, w_gate_hbm, state_hbm,
     out_ref, state,
-    w_in, w_val, w_gate, b_re, b_im, c_re, c_im, drive, read,
+    stream_ref, gain_ref, lam_re_ref, lam_im_ref, log_dt_ref, skip_ref, own_w, b_re, b_im, c_re, c_im, drive, read,
     kept, proj, u_keep, masked, from_old, mix_w,
     x_all, part_send, part_recv, sq_send, sq_recv, mix_all, comb_send, comb_own, comb_recv,
-    gain_all, far_in, far_val, far_gate, x_far, swap_send, swap_recv, u_send, u_recv, out_send, out_recv,
-    load_sem, x_ss, x_rs, part_ss, part_rs, sq_ss, sq_rs, mix_ss, mix_rs, comb_ss, comb_rs,
-    gain_ss, gain_rs, far_ss, far_rs, xf_ss, xf_rs, swap_ss, swap_rs, u_ss, u_rs, of_ss, of_rs,
+    gain_all, col_w, far_w, x_far, swap_send, swap_recv, u_send, u_recv, out_send, out_recv,
+    small_sem, load_sem, x_ss, x_rs, part_ss, part_rs, sq_ss, sq_rs, mix_ss, mix_rs, comb_ss, comb_rs,
+    gain_ss, gain_rs, col_ss, col_rs, row_ss, row_rs, xf_ss, xf_rs, swap_ss, swap_rs, u_ss, u_rs, of_ss, of_rs,
 ):
-    layers = w_in.shape[0]
+    layers = w_in_hbm.shape[0]
     me_t, me_d = lax.axis_index("tp"), lax.axis_index("dp")
     rows_t, feats = stream_ref.shape
     rows_d, width = u_keep.shape
@@ -49,17 +49,6 @@
     sq_width = sq_send.shape[2]
     me_z, me_y = me_t // per, me_t % per
 
-    loads = {}
-    for l in range(layers):
-        for i, (src, dst) in enumerate(
-            (
-                (b_re_hbm, b_re), (b_im_hbm, b_im), (c_re_hbm, c_re), (c_im_hbm, c_im), (state_hbm, state),
-                (w_in_hbm, w_in), (w_val_hbm, w_val), (w_gate_hbm, w_gate),
-            )
-        ):
-            loads[l, i] = pltpu.make_async_copy(src.at[l], dst.at[l], load_sem.at[l, i])
-            loads[l, i].start()
-
     barrier = pltpu.get_barrier_semaphore()
 
     def greet(t, d):
@@ -72,11 +61,32 @@
     for j in range(1, per):
         for k in range(1, dp):
             greet(me_z * per + partner(me_y, j, per), partner(me_d, k, dp))
-    for k in range(dp):
-
-        @pl.when(jnp.logical_or(me_z != me_d, k != me_d))
-        def _():
-            greet(me_d * per + me_y, k)
+
+    @pl.when(me_z != me_d)
+    def _():
+        greet(me_d * per + me_y, me_z)
+
+    smalls = []
+    for i, (src, dst) in enumerate(
+        (
+            (stream_hbm, stream_ref), (gain_hbm, gain_ref), (lam_re_hbm, lam_re_ref), (lam_im_hbm, lam_im_ref),
+            (log_dt_hbm, log_dt_ref), (skip_hbm, skip_ref),
+        )
+    ):
+        smalls.append(pltpu.make_async_copy(src, dst, small_sem.at[i]))
+        smalls[i].start()
+    loads = {}
+    for l in range(layers):
+        weights = own_w if l == 0 else col_w.at[me_z]
+        for i, (src, dst) in enumerate(
+            (
+                (b_re_hbm, b_re.at[l]), (b_im_hbm, b_im.at[l]), (c_re_hbm, c_re.at[l]), (c_im_hbm, c_im.at[l]),
+                (state_hbm, state.at[l]), (w_in_hbm, weights.at[0]), (w_val_hbm, weights.at[1]),
+                (w_gate_hbm, weights.at[2]),
+            )
+        ):
+            loads[l, i] = pltpu.make_async_copy(src.at[l], dst, load_sem.at[l, i])
+            loads[l, i].start()
 
     def send(src, dst, ss, rs, t, d):
         return pltpu.make_async_remote_copy(
@@ -103,10 +113,37 @@
     def gain_copy(to):
         return send(gain_all.at[me_d], gain_all.at[me_d], gain_ss.at[to], gain_rs.at[me_d], me_t, to)
 
-    far = ((w_in, far_in), (w_val, far_val), (w_gate, far_gate))
-
-    def far_copy(i, z):
-        return send(far[i][0].at[1], far[i][1].at[me_d], far_ss.at[i, z], far_rs.at[i, me_d], z * per + me_y, me_z)
+    def col_copy(side, i):
+        sign = 1 - 2 * side
+        home = lax.rem(me_z - sign * min(i - 1, 2) + 2 * dp, dp)
+        to = lax.rem(me_z + sign * (2 if i == 4 else 1) + dp, dp)
+        part = col_w.at[home]
+        if i == 4:
+            part = part.at[:, pl.ds(side * (width // 2), width // 2)]
+        return send(part, part, col_ss.at[side, i - 1], col_rs.at[side, i - 1], to * per + me_y, me_d)
+
+    def col_wait(side, i):
+        home = lax.rem(me_z - (1 - 2 * side) * i + 2 * dp, dp)
+        part = col_w.at[home]
+        if i == 4:
+            part = part.at[:, pl.ds(side * (width // 2), width // 2)]
+        arrival(part, col_rs.at[side, i - 1]).wait_recv()
+
+    def row_copy(z, i):
+        some = pl.ds(0, 1) if i == 0 else pl.ds(1, 2)
+        return send(col_w.at[z, some], far_w.at[me_d, some], row_ss.at[i, z], row_rs.at[i, me_d], me_t, z)
+
+    def row_wait(d, i):
+        some = pl.ds(0, 1) if i == 0 else pl.ds(1, 2)
+        arrival(far_w.at[d, some], row_rs.at[i, d]).wait_recv()
+
+    def row_start(step):
+        for i in range(2):
+            z = lax.rem(me_z + step + dp, dp)
+
+            @pl.when(z != me_d)
+            def _():
+                row_copy(z, i).start()
 
     def xf_copy(y, d):
         return send(x_far.at[me_d, me_y], x_far.at[me_d, me_y], xf_ss.at[d, y], xf_rs.at[me_d, me_y], me_z * per + y, d)
@@ -122,24 +159,6 @@
 
     def arrival(ref, rs):
         return send(ref, ref, rs, rs, 0, 0)
-
-    def spread(i):
-        loads[1, 5 + i].wait()
-        for k in reversed(range(dp)):
-            z = partner(me_z, k, dp)
-
-            @pl.when(jnp.logical_or(z != me_z, me_z != me_d))
-            def _():
-                far_copy(i, z).start()
-
-        @pl.when(me_z == me_d)
-        def _():
-            far[i][1][me_d] = far[i][0][1]
-
-    def spread_wait(i, d):
-        @pl.when(jnp.logical_or(d != me_d, me_z != me_d))
-        def _():
-            arrival(far[i][1].at[d], far_rs.at[i, d]).wait_recv()
 
     lane_group = lax.broadcasted_iota(jnp.int32, (rows_d, width), 1) // chans
     eye = lax.broadcasted_iota(jnp.int32, (rows_d, sq_width), 0) == lax.broadcasted_iota(jnp.int32, (rows_d, sq_width), 1)
@@ -190,21 +209,32 @@
             state[l, pl.ds(g, rows_d, stride=groups), :] = kept[l, pl.ds(g * rows_d, rows_d), :]
 
     elsewhere = ((me_z - me_d) * (me_z - me_d) + dp * dp - 1) // (dp * dp)
-    pl.semaphore_wait(barrier, tp - 1 + dp - 1 + (per - 1) * (dp - 1) + dp - 1 + elsewhere)
-
+    pl.semaphore_wait(barrier, tp - 1 + dp - 1 + (per - 1) * (dp - 1) + elsewhere)
+
+    smalls[0].wait()
     for k in reversed(range(1, tp)):
         x_copy(k).start()
+    smalls[1].wait()
     gain_all[me_d] = jnp.broadcast_to(gain_ref[1:2, :], (rows_t, feats))
     for k in reversed(range(1, dp)):
         gain_copy(partner(me_d, k, dp)).start()
-    spread(0)
+    for i in range(5, 8):
+        loads[1, i].wait()
+    for side in range(2):
+        col_copy(side, 1).start()
     x_all[me_t] = stream_ref[...]
+    for small in smalls[2:]:
+        small.wait()
     from_old[...], mix_w[...] = prepare(0)
 
     loads[0, 5].wait()
     gain = gain_ref[0:1, :]
     own_part = own_sq = None
     for k in reversed(range(dp)):
+        if k == 1:
+            for side in range(2):
+                col_wait(side, 1)
+                col_copy(side, 2).start()
         to = partner(me_d, k, dp)
         for j in range(per):
             t = to * per + j
@@ -216,7 +246,7 @@
         x = x_all[pl.ds(to * per, per)].astype(F32).reshape(rows_d, feats)
         column = jnp.sum(x * x, axis=1, keepdims=True)
         squares = jnp.sum(jnp.where(eye, column, 0.0), axis=0, keepdims=True)
-        product = lax.dot_general((x * gain).astype(BF16), w_in[0], NT, preferred_element_type=F32)
+        product = lax.dot_general((x * gain).astype(BF16), own_w[0], NT, preferred_element_type=F32)
         if k:
             sq_send[to] = jnp.broadcast_to(squares, (8, sq_width))
             sq_copy(to).start()
@@ -224,7 +254,6 @@
             part_copy(to).start()
         else:
             own_part, own_sq = product, squares
-    spread(1)
     for k in range(1, dp):
         by = partner(me_d, k, dp, True)
         arrival(sq_recv.at[by], sq_rs.at[by]).wait_recv()
@@ -238,6 +267,10 @@
     mix_all[me_d] = jax.nn.gelu(pre).astype(BF16)
     for k in reversed(range(1, dp)):
         mix_copy(partner(me_d, k, dp)).start()
+    for side in range(2):
+        col_wait(side, 2)
+        col_copy(side, 3).start()
+        col_copy(side, 4).start()
     loads[0, 6].wait()
     loads[0, 7].wait()
     for k in range(dp):
@@ -245,8 +278,8 @@
         if k:
             arrival(mix_all.at[by], mix_rs.at[by]).wait_recv()
         mixed = mix_all[by]
-        value = jnp.dot(mixed, w_val[0], preferred_element_type=F32)
-        gate = jnp.dot(mixed, w_gate[0], preferred_element_type=F32)
+        value = jnp.dot(mixed, own_w[1], preferred_element_type=F32)
+        gate = jnp.dot(mixed, own_w[2], preferred_element_type=F32)
         for j in range(per):
             t = by * per + j
             rows = slice(j * rows_t, (j + 1) * rows_t)
@@ -262,7 +295,8 @@
                 comb_own[:, :feats] = value[rows]
                 comb_own[:, feats:] = gate[rows]
 
-    spread(2)
+    for step in (0, 1, -1, 2, -2):
+        row_start(step)
     update(0, u_keep[...])
     total, mixer = prepare(1)
     swap_send[:rows_d] = jnp.concatenate([total, total], axis=1)
@@ -275,6 +309,23 @@
     @pl.when(me_z == me_d)
     def _():
         swap_recv[...] = swap_send[...]
+
+    for side in range(2):
+        col_wait(side, 3)
+        col_wait(side, 4)
+    for step in (3, -3, 4):
+        row_start(step)
+    for k in range(1, tp):
+        x_copy(k).wait_send()
+    for k in range(1, dp):
+        to = partner(me_d, k, dp)
+        part_copy(to).wait_send()
+        sq_copy(to).wait_send()
+        mix_copy(to).wait_send()
+        gain_copy(to).wait_send()
+    for side in range(2):
+        for i in range(1, 5):
+            col_copy(side, i).wait_send()
 
     combined = comb_own[...]
     for k in range(1, tp):
@@ -288,6 +339,13 @@
         for j in ROW_FAR_FIRST:
             if k or j:
                 xf_copy(partner(me_y, j, per), partner(me_d, k, dp)).start()
+    for k in range(1, tp):
+        comb_copy(partner(me_t, k, tp)).wait_send()
+
+    @pl.when(me_z != me_d)
+    def _():
+        swap_copy().wait_send()
+
     for k in range(1, dp):
         by = partner(me_d, k, dp, True)
         arrival(gain_all.at[by], gain_rs.at[by]).wait_recv()
@@ -296,7 +354,9 @@
     squares = jnp.zeros((rows_d, feats), F32)
     for k in reversed(PLANE_FAR_FIRST):
         by = partner(me_d, k, dp, True)
-        spread_wait(0, by)
+        if k:
+            row_wait(by, 0)
+        weights = far_w.at[by] if k else col_w.at[me_d]
         for j in reversed(ROW_FAR_FIRST):
             if k or j:
                 y = partner(me_y, j, per)
@@ -305,7 +365,7 @@
         normed = (x * gain_all[by][None]).astype(BF16).reshape(rows_d, feats)
         x = x.reshape(rows_d, feats)
         squares = squares + x * x
-        acc = acc + lax.dot_general(normed, far_in[by], NT, preferred_element_type=F32)
+        acc = acc + lax.dot_general(normed, weights[0], NT, preferred_element_type=F32)
     u = lax.rsqrt(jnp.sum(squares, axis=1, keepdims=True) / (feats * dp) + EPS) * acc
     u_send[...] = jnp.concatenate([u, u], axis=1)
 
@@ -324,15 +384,20 @@
     mixed = jax.nn.gelu(pre).astype(BF16)
     for k in PLANE_FAR_FIRST:
         to = partner(me_d, k, dp)
-        spread_wait(1, to)
-        spread_wait(2, to)
-        value = jnp.dot(mixed, far_val[to], preferred_element_type=F32)
-        gate = jnp.dot(mixed, far_gate[to], preferred_element_type=F32)
+        if k:
+            row_wait(to, 1)
+        weights = far_w.at[to] if k else col_w.at[me_d]
+        value = jnp.dot(mixed, weights[1], preferred_element_type=F32)
+        gate = jnp.dot(mixed, weights[2], preferred_element_type=F32)
         out_send[to, :, :, :feats] = value.astype(BF16).reshape(per, rows_t, feats)
         out_send[to, :, :, feats:] = gate.astype(BF16).reshape(per, rows_t, feats)
         for j in ROW_FAR_FIRST:
             if k or j:
                 of_copy(partner(me_y, j, per), to).start()
+    for k in range(dp):
+        for j in range(per):
+            if k or j:
+                xf_copy(partner(me_y, j, per), partner(me_d, k, dp)).wait_send()
     combined = out_send[me_d, me_y].astype(F32)
 
     @pl.when(me_z != me_d)
@@ -351,32 +416,16 @@
         x_far[me_d, me_y].astype(F32) + combined[:, :feats] * jax.nn.sigmoid(combined[:, feats:])
     ).astype(BF16)
 
-    for k in range(1, tp):
-        x_copy(k).wait_send()
-        comb_copy(partner(me_t, k, tp)).wait_send()
-    for k in range(1, dp):
-        to = partner(me_d, k, dp)
-        part_copy(to).wait_send()
-        sq_copy(to).wait_send()
-        mix_copy(to).wait_send()
-        gain_copy(to).wait_send()
-    for k in range(dp):
-        z = partner(me_z, k, dp)
-
-        @pl.when(jnp.logical_or(z != me_z, me_z != me_d))
-        def _():
-            for i in range(3):
-                far_copy(i, z).wait_send()
-
     for k in range(dp):
         for j in range(per):
             if k or j:
-                xf_copy(partner(me_y, j, per), partner(me_d, k, dp)).wait_send()
                 of_copy(partner(me_y, j, per), partner(me_d, k, dp)).wait_send()
+    for k in range(1, dp):
+        for i in range(2):
+            row_copy(partner(me_d, k, dp), i).wait_send()
 
     @pl.when(me_z != me_d)
     def _():
-        swap_copy().wait_send()
         u_copy().wait_send()
 
 
@@ -402,12 +451,16 @@
     out, states = pl.pallas_call(
         functools.partial(kernel, tp, dp, chans),
         out_shape=(pltpu.VMEM(stream.shape, BF16), pltpu.VMEM((layers, rows_d * groups, lanes), F32)),
-        in_specs=[vmem, vmem, hbm, vmem, vmem, vmem, hbm, hbm, hbm, hbm, vmem, hbm, hbm, hbm],
+        in_specs=[hbm] * 14,
         out_specs=(vmem, vmem),
         scratch_shapes=[
-            pltpu.VMEM(turned_in.shape, BF16),
-            pltpu.VMEM(w_val.shape, BF16),
-            pltpu.VMEM(w_gate.shape, BF16),
+            pltpu.VMEM(stream.shape, BF16),
+            pltpu.VMEM(norm_gain.shape, F32),
+            pltpu.VMEM(lam_re.shape, F32),
+            pltpu.VMEM(lam_im.shape, F32),
+            pltpu.VMEM(log_dt.shape, F32),
+            pltpu.VMEM(d_skip.shape, F32),
+            pltpu.VMEM((3, width, feats), BF16),
             pltpu.VMEM(turned_re.shape, F32),
             pltpu.VMEM(turned_im.shape, F32),
             pltpu.VMEM(readout_real.shape, F32),
@@ -430,9 +483,8 @@
             pltpu.VMEM((rows_t, 2 * feats), F32),
             pltpu.VMEM((tp, rows_t, 2 * feats), BF16),
             pltpu.VMEM((dp, rows_t, feats), F32),
-            pltpu.VMEM((dp, width, feats), BF16),
-            pltpu.VMEM((dp, width, feats), BF16),
-            pltpu.VMEM((dp, width, feats), BF16),
+            pltpu.VMEM((dp, 3, width, feats), BF16),
+            pltpu.VMEM((dp, 3, width, feats), BF16),
             pltpu.VMEM((dp, per, rows_t, feats), BF16),
             pltpu.VMEM((rows_d + width, 128), F32),
             pltpu.VMEM((rows_d + width, 128), F32),
@@ -440,14 +492,15 @@
             pltpu.VMEM((rows_d, 128), F32),
             pltpu.VMEM((dp, per, rows_t, 2 * feats), BF16),
             pltpu.VMEM((dp, per, rows_t, 2 * feats), BF16),
-            dma(layers, 8),
+            dma(6), dma(layers, 8),
             dma(tp), dma(tp),
             dma(dp), dma(dp),
             dma(dp), dma(dp),
             dma(dp), dma(dp),
             dma(tp), dma(tp),
             dma(dp), dma(dp),
-            dma(3, dp), dma(3, dp),
+            dma(2, 4), dma(2, 4),
+            dma(2, dp), dma(2, dp),
             dma(dp, per), dma(dp, per),
             pltpu.SemaphoreType.DMA, pltpu.SemaphoreType.DMA,
             pltpu.SemaphoreType.DMA, pltpu.SemaphoreType.DMA,

time: 57 us -> 55.5 us (0.974)
  Pallas kernels: 55 us -> 53.4 us
    pallas_call x1, Pallas kernels: 55 us -> 53.4 us  [per_device(): pl.pallas_call(functools.partial(kernel, tp, dp, chans), out_shape=(pltpu...]
where the time goes in v2:
time: 55.5 us; the launch traced here: 55.3 us
  Pallas kernels  53.4 us (96%)
  local copies, waits for them, and re-layouts  1.25 us (2%)
  between operations  0.64 us (1%)
    pallas_call x1, Pallas kernels, per_device(): pl.pallas_call(functools.partial(kernel, tp, dp, chans), out_shape=(pltpu...  53.4 us
    unnamed x2, local copies, waits for them, and re-layouts  1.25 us

profile of v2, /device:TPU:1, one launch (start us, length us, event | category | flops | bytes accessed | tf_op | source)
XLA Modules:
  0.0 55.3 jit_solution(14330468491299065048)
XLA Ops:
  0.6 53.4 %shard_map.149 = (bf16[8,256]{1,0:T(8,128)(2,1)S(1)}, f32[2,128,128]{2,1,0:T(8,128)S(1)}) custom-call(bf16[8,256]{1,0:T(8,128)(2,1)} %stream_hbm.1, f32[2,256]{1,0:T(2,128)} %gain_hbm.1, bf16[2,64,256]{2,1,0:T(8,128)(2,1)} %bitcast.7, f32[2,4,64]{2,1,0:T(4,128)} %lam_re_hbm.1, f32[2,4,64]{2,1,0:T(4,128)} %lam_im_hbm.1, f32[2,4]{1,0:T(2,128)} %log_dt_hbm.1, ...), custom_call_target="tpu_custom_call" | custom-call | tf_op jit(solution)/shard_map/pallas_call | solution.py:451
  54.1 0.6 %copy.18 = bf16[8,256]{1,0:T(8,128)(2,1)} copy(bf16[8,256]{1,0:T(8,128)(2,1)S(1)} %get-tuple-element.6) | data formatting | bytes 8192
  54.7 0.7 %copy.19 = f32[2,32,4,128]{3,2,1,0:T(4,128)} copy(f32[2,32,4,128]{3,2,1,0:T(4,128)S(1)} %bitcast.5) | data formatting | bytes 262144

commit v3 on v2

--- a/solution.py
+++ b/solution.py
@@ -34,10 +34,10 @@
     out_ref, state,
     stream_ref, gain_ref, lam_re_ref, lam_im_ref, log_dt_ref, skip_ref, own_w, b_re, b_im, c_re, c_im, drive, read,
     kept, proj, u_keep, masked, from_old, mix_w,
-    x_all, part_send, part_recv, sq_send, sq_recv, mix_all, comb_send, comb_own, comb_recv,
-    gain_all, col_w, far_w, x_far, swap_send, swap_recv, u_send, u_recv, out_send, out_recv,
-    small_sem, load_sem, x_ss, x_rs, part_ss, part_rs, sq_ss, sq_rs, mix_ss, mix_rs, comb_ss, comb_rs,
-    gain_ss, gain_rs, col_ss, col_rs, row_ss, row_rs, xf_ss, xf_rs, swap_ss, swap_rs, u_ss, u_rs, of_ss, of_rs,
+    x_all, part_send, part_recv, sq_send, sq_recv, mix_all, near_own, near_send, near_recv, comb_send, comb_own, comb_recv,
+    gain_all, col_in, col_out, far_in, x_far, swap_send, swap_recv, u_send, u_recv, mix_far, out_send, out_recv,
+    small_sem, load_sem, x_ss, x_rs, part_ss, part_rs, sq_ss, sq_rs, mix_ss, mix_rs, near_ss, near_rs, comb_ss, comb_rs,
+    gain_ss, gain_rs, col_ss, col_rs, row_ss, row_rs, xf_ss, xf_rs, swap_ss, swap_rs, u_ss, u_rs, mf_ss, mf_rs, of_ss, of_rs,
 ):
     layers = w_in_hbm.shape[0]
     me_t, me_d = lax.axis_index("tp"), lax.axis_index("dp")
@@ -77,12 +77,13 @@
         smalls[i].start()
     loads = {}
     for l in range(layers):
-        weights = own_w if l == 0 else col_w.at[me_z]
+        weights = (
+            [own_w.at[i] for i in range(3)] if l == 0 else [col_in.at[me_z], col_out.at[me_z, 0], col_out.at[me_z, 1]]
+        )
         for i, (src, dst) in enumerate(
             (
                 (b_re_hbm, b_re.at[l]), (b_im_hbm, b_im.at[l]), (c_re_hbm, c_re.at[l]), (c_im_hbm, c_im.at[l]),
-                (state_hbm, state.at[l]), (w_in_hbm, weights.at[0]), (w_val_hbm, weights.at[1]),
-                (w_gate_hbm, weights.at[2]),
+                (state_hbm, state.at[l]), (w_in_hbm, weights[0]), (w_val_hbm, weights[1]), (w_gate_hbm, weights[2]),
             )
         ):
             loads[l, i] = pltpu.make_async_copy(src.at[l], dst, load_sem.at[l, i])
@@ -107,49 +108,51 @@
     def mix_copy(to):
         return send(mix_all.at[me_d], mix_all.at[me_d], mix_ss.at[to], mix_rs.at[me_d], me_t, to)
 
-    def comb_copy(to):
-        return send(comb_send.at[to], comb_recv.at[me_t], comb_ss.at[to], comb_rs.at[me_t], to, me_d)
+    def near_copy(z, y):
+        return send(
+            near_send.at[z, y], near_recv.at[z, me_y], near_ss.at[z, y], near_rs.at[z, me_y], me_z * per + y, me_d
+        )
+
+    def comb_copy(z):
+        return send(comb_send.at[z], comb_recv.at[me_z], comb_ss.at[z], comb_rs.at[me_z], z * per + me_y, me_d)
 
     def gain_copy(to):
         return send(gain_all.at[me_d], gain_all.at[me_d], gain_ss.at[to], gain_rs.at[me_d], me_t, to)
 
-    def col_copy(side, i):
+    def col_part(what, home, side, i):
+        if what:
+            return col_out.at[home, :, pl.ds(side * (width // 2), width // 2)] if i == 4 else col_out.at[home]
+        return col_in.at[home, pl.ds(side * (width // 2), width // 2)] if i == 4 else col_in.at[home]
+
+    def col_copy(what, side, i):
         sign = 1 - 2 * side
         home = lax.rem(me_z - sign * min(i - 1, 2) + 2 * dp, dp)
         to = lax.rem(me_z + sign * (2 if i == 4 else 1) + dp, dp)
-        part = col_w.at[home]
-        if i == 4:
-            part = part.at[:, pl.ds(side * (width // 2), width // 2)]
-        return send(part, part, col_ss.at[side, i - 1], col_rs.at[side, i - 1], to * per + me_y, me_d)
-
-    def col_wait(side, i):
-        home = lax.rem(me_z - (1 - 2 * side) * i + 2 * dp, dp)
-        part = col_w.at[home]
-        if i == 4:
-            part = part.at[:, pl.ds(side * (width // 2), width // 2)]
-        arrival(part, col_rs.at[side, i - 1]).wait_recv()
-
-    def row_copy(z, i):
-        some = pl.ds(0, 1) if i == 0 else pl.ds(1, 2)
-        return send(col_w.at[z, some], far_w.at[me_d, some], row_ss.at[i, z], row_rs.at[i, me_d], me_t, z)
-
-    def row_wait(d, i):
-        some = pl.ds(0, 1) if i == 0 else pl.ds(1, 2)
-        arrival(far_w.at[d, some], row_rs.at[i, d]).wait_recv()
-
-    def row_start(step):
-        for i in range(2):
-            z = lax.rem(me_z + step + dp, dp)
-
-            @pl.when(z != me_d)
-            def _():
-                row_copy(z, i).start()
+        part = col_part(what, home, side, i)
+        return send(part, part, col_ss.at[what, side, i - 1], col_rs.at[what, side, i - 1], to * per + me_y, me_d)
+
+    def col_start(what, *hops):
+        for i in hops:
+            for side in range(2):
+                col_copy(what, side, i).start()
+
+    def col_wait(what, *hops):
+        for i in hops:
+            for side in range(2):
+                home = lax.rem(me_z - (1 - 2 * side) * i + 2 * dp, dp)
+                arrival(col_part(what, home, side, i), col_rs.at[what, side, i - 1]).wait_recv()
+
+    def row_copy(z):
+        return send(col_in.at[z], far_in.at[me_d], row_ss.at[z], row_rs.at[me_d], me_t, z)
+
+    def mf_copy(to):
+        return send(mix_far.at[me_d], mix_far.at[me_d], mf_ss.at[to], mf_rs.at[me_d], me_t, to)
 
     def xf_copy(y, d):
         return send(x_far.at[me_d, me_y], x_far.at[me_d, me_y], xf_ss.at[d, y], xf_rs.at[me_d, me_y], me_z * per + y, d)
 
-    def of_copy(y, d):
-        return send(out_send.at[d, y], out_recv.at[me_d, me_y], of_ss.at[d, y], of_rs.at[me_d, me_y], me_z * per + y, d)
+    def of_copy(y):
+        return send(out_send.at[y], out_recv.at[me_y], of_ss.at[y], of_rs.at[me_y], me_z * per + y, me_d)
 
     def swap_copy():
         return send(swap_send, swap_recv, swap_ss, swap_rs, me_d * per + me_y, me_z)
@@ -218,10 +221,8 @@
     gain_all[me_d] = jnp.broadcast_to(gain_ref[1:2, :], (rows_t, feats))
     for k in reversed(range(1, dp)):
         gain_copy(partner(me_d, k, dp)).start()
-    for i in range(5, 8):
-        loads[1, i].wait()
-    for side in range(2):
-        col_copy(side, 1).start()
+    loads[1, 5].wait()
+    col_start(0, 1)
     x_all[me_t] = stream_ref[...]
     for small in smalls[2:]:
         small.wait()
@@ -231,10 +232,9 @@
     gain = gain_ref[0:1, :]
     own_part = own_sq = None
     for k in reversed(range(dp)):
-        if k == 1:
-            for side in range(2):
-                col_wait(side, 1)
-                col_copy(side, 2).start()
+        if k == 6:
+            col_wait(0, 1)
+            col_start(0, 2)
         to = partner(me_d, k, dp)
         for j in range(per):
             t = to * per + j
@@ -254,12 +254,18 @@
             part_copy(to).start()
         else:
             own_part, own_sq = product, squares
+    loads[1, 6].wait()
+    loads[1, 7].wait()
+    col_start(1, 1)
     for k in range(1, dp):
         by = partner(me_d, k, dp, True)
         arrival(sq_recv.at[by], sq_rs.at[by]).wait_recv()
         own_sq = own_sq + sq_recv[by][0:1, :]
         arrival(part_recv.at[by], part_rs.at[by]).wait_recv()
         own_part = own_part + part_recv[by].astype(F32)
+        if k == 2:
+            col_wait(0, 2)
+            col_start(0, 3, 4)
     square_total = jnp.sum(jnp.where(eye, own_sq, 0.0), axis=1, keepdims=True)
     u = lax.rsqrt(square_total / (feats * dp) + EPS) * own_part
     u_keep[...] = u
@@ -267,10 +273,6 @@
     mix_all[me_d] = jax.nn.gelu(pre).astype(BF16)
     for k in reversed(range(1, dp)):
         mix_copy(partner(me_d, k, dp)).start()
-    for side in range(2):
-        col_wait(side, 2)
-        col_copy(side, 3).start()
-        col_copy(side, 4).start()
     loads[0, 6].wait()
     loads[0, 7].wait()
     for k in range(dp):
@@ -280,23 +282,36 @@
         mixed = mix_all[by]
         value = jnp.dot(mixed, own_w[1], preferred_element_type=F32)
         gate = jnp.dot(mixed, own_w[2], preferred_element_type=F32)
-        for j in range(per):
-            t = by * per + j
-            rows = slice(j * rows_t, (j + 1) * rows_t)
-
-            @pl.when(t != me_t)
-            def _():
-                comb_send[t, :, :feats] = value[rows].astype(BF16)
-                comb_send[t, :, feats:] = gate[rows].astype(BF16)
-                comb_copy(t).start()
-
-            @pl.when(t == me_t)
-            def _():
-                comb_own[:, :feats] = value[rows]
-                comb_own[:, feats:] = gate[rows]
-
-    for step in (0, 1, -1, 2, -2):
-        row_start(step)
+        near_own[by, :, :, :feats] = value.reshape(per, rows_t, feats)
+        near_own[by, :, :, feats:] = gate.reshape(per, rows_t, feats)
+        near_send[by, :, :, :feats] = value.astype(BF16).reshape(per, rows_t, feats)
+        near_send[by, :, :, feats:] = gate.astype(BF16).reshape(per, rows_t, feats)
+        for j in ROW_FAR_FIRST:
+            if j:
+                near_copy(by, partner(me_y, j, per)).start()
+
+    def gather_near(k):
+        z = partner(me_d, k, dp, True)
+        total = near_own[z, me_y]
+        for j in range(1, per):
+            y = partner(me_y, j, per)
+            arrival(near_recv.at[z, y], near_rs.at[z, y]).wait_recv()
+            total = total + near_recv[z, y].astype(F32)
+
+        @pl.when(z != me_z)
+        def _():
+            comb_send[z] = total.astype(BF16)
+            comb_copy(z).start()
+
+        @pl.when(z == me_z)
+        def _():
+            comb_own[...] = total
+
+    col_wait(0, 3, 4)
+    for k in reversed(range(1, dp)):
+        row_copy(partner(me_d, k, dp)).start()
+    for k in range(4):
+        gather_near(k)
     update(0, u_keep[...])
     total, mixer = prepare(1)
     swap_send[:rows_d] = jnp.concatenate([total, total], axis=1)
@@ -310,11 +325,8 @@
     def _():
         swap_recv[...] = swap_send[...]
 
-    for side in range(2):
-        col_wait(side, 3)
-        col_wait(side, 4)
-    for step in (3, -3, 4):
-        row_start(step)
+    for k in range(4, dp):
+        gather_near(k)
     for k in range(1, tp):
         x_copy(k).wait_send()
     for k in range(1, dp):
@@ -325,11 +337,13 @@
         gain_copy(to).wait_send()
     for side in range(2):
         for i in range(1, 5):
-            col_copy(side, i).wait_send()
-
+            col_copy(0, side, i).wait_send()
+
+    col_wait(1, 1)
+    col_start(1, 2)
     combined = comb_own[...]
-    for k in range(1, tp):
-        by = partner(me_t, k, tp, True)
+    for k in range(1, dp):
+        by = partner(me_z, k, dp, True)
         arrival(comb_recv.at[by], comb_rs.at[by]).wait_recv()
         combined = combined + comb_recv[by].astype(F32)
     fresh = (x_all[me_t].astype(F32) + combined[:, :feats] * jax.nn.sigmoid(combined[:, feats:])).astype(BF16)
@@ -339,8 +353,11 @@
         for j in ROW_FAR_FIRST:
             if k or j:
                 xf_copy(partner(me_y, j, per), partner(me_d, k, dp)).start()
-    for k in range(1, tp):
-        comb_copy(partner(me_t, k, tp)).wait_send()
+    for k in range(1, dp):
+        comb_copy(partner(me_z, k, dp)).wait_send()
+    for k in range(dp):
+        for j in range(1, per):
+            near_copy(k, partner(me_y, j, per)).wait_send()
 
     @pl.when(me_z != me_d)
     def _():
@@ -354,9 +371,12 @@
     squares = jnp.zeros((rows_d, feats), F32)
     for k in reversed(PLANE_FAR_FIRST):
         by = partner(me_d, k, dp, True)
+        if k == 3:
+            col_wait(1, 2)
+            col_start(1, 3, 4)
         if k:
-            row_wait(by, 0)
-        weights = far_w.at[by] if k else col_w.at[me_d]
+            arrival(far_in.at[by], row_rs.at[by]).wait_recv()
+        weights = far_in.at[by] if k else col_in.at[me_d]
         for j in reversed(ROW_FAR_FIRST):
             if k or j:
                 y = partner(me_y, j, per)
@@ -365,7 +385,7 @@
         normed = (x * gain_all[by][None]).astype(BF16).reshape(rows_d, feats)
         x = x.reshape(rows_d, feats)
         squares = squares + x * x
-        acc = acc + lax.dot_general(normed, weights[0], NT, preferred_element_type=F32)
+        acc = acc + lax.dot_general(normed, weights[...], NT, preferred_element_type=F32)
     u = lax.rsqrt(jnp.sum(squares, axis=1, keepdims=True) / (feats * dp) + EPS) * acc
     u_send[...] = jnp.concatenate([u, u], axis=1)
 
@@ -381,48 +401,56 @@
     pre = swap_recv[:rows_d, :width] + jnp.dot(
         u, swap_recv[rows_d:, :width], precision=HIGHEST, preferred_element_type=F32
     )
-    mixed = jax.nn.gelu(pre).astype(BF16)
+    mix_far[me_d] = jax.nn.gelu(pre).astype(BF16)
     for k in PLANE_FAR_FIRST:
-        to = partner(me_d, k, dp)
         if k:
-            row_wait(to, 1)
-        weights = far_w.at[to] if k else col_w.at[me_d]
-        value = jnp.dot(mixed, weights[1], preferred_element_type=F32)
-        gate = jnp.dot(mixed, weights[2], preferred_element_type=F32)
-        out_send[to, :, :, :feats] = value.astype(BF16).reshape(per, rows_t, feats)
-        out_send[to, :, :, feats:] = gate.astype(BF16).reshape(per, rows_t, feats)
-        for j in ROW_FAR_FIRST:
-            if k or j:
-                of_copy(partner(me_y, j, per), to).start()
+            mf_copy(partner(me_d, k, dp)).start()
+    col_wait(1, 3, 4)
     for k in range(dp):
         for j in range(per):
             if k or j:
                 xf_copy(partner(me_y, j, per), partner(me_d, k, dp)).wait_send()
-    combined = out_send[me_d, me_y].astype(F32)
-
-    @pl.when(me_z != me_d)
-    def _():
-        arrival(u_recv, u_rs).wait_recv()
-
-    update(1, u_recv[:, :width])
+    for k in range(1, dp):
+        row_copy(partner(me_d, k, dp)).wait_send()
+    for side in range(2):
+        for i in range(1, 5):
+            col_copy(1, side, i).wait_send()
+    value = jnp.zeros((rows_d, feats), F32)
+    gate = jnp.zeros((rows_d, feats), F32)
     for k in reversed(PLANE_FAR_FIRST):
         by = partner(me_d, k, dp, True)
-        for j in reversed(ROW_FAR_FIRST):
-            if k or j:
-                y = partner(me_y, j, per)
-                arrival(out_recv.at[by, y], of_rs.at[by, y]).wait_recv()
-                combined = combined + out_recv[by, y].astype(F32)
+        if k:
+            arrival(mix_far.at[by], mf_rs.at[by]).wait_recv()
+        mixed = mix_far[by]
+        value = value + jnp.dot(mixed, col_out[by, 0], preferred_element_type=F32)
+        gate = gate + jnp.dot(mixed, col_out[by, 1], preferred_element_type=F32)
+    near_own[0, :, :, :feats] = value.reshape(per, rows_t, feats)
+    near_own[0, :, :, feats:] = gate.reshape(per, rows_t, feats)
+    out_send[:, :, :feats] = value.astype(BF16).reshape(per, rows_t, feats)
+    out_send[:, :, feats:] = gate.astype(BF16).reshape(per, rows_t, feats)
+    for j in ROW_FAR_FIRST:
+        if j:
+            of_copy(partner(me_y, j, per)).start()
+
+    @pl.when(me_z != me_d)
+    def _():
+        arrival(u_recv, u_rs).wait_recv()
+
+    update(1, u_recv[:, :width])
+    combined = near_own[0, me_y]
+    for j in reversed(ROW_FAR_FIRST):
+        if j:
+            y = partner(me_y, j, per)
+            arrival(out_recv.at[y], of_rs.at[y]).wait_recv()
+            combined = combined + out_recv[y].astype(F32)
     out_ref[...] = (
         x_far[me_d, me_y].astype(F32) + combined[:, :feats] * jax.nn.sigmoid(combined[:, feats:])
     ).astype(BF16)
 
-    for k in range(dp):
-        for j in range(per):
-            if k or j:
-                of_copy(partner(me_y, j, per), partner(me_d, k, dp)).wait_send()
-    for k in range(1, dp):
-        for i in range(2):
-            row_copy(partner(me_d, k, dp), i).wait_send()
+    for k in range(1, dp):
+        mf_copy(partner(me_d, k, dp)).wait_send()
+    for j in range(1, per):
+        of_copy(partner(me_y, j, per)).wait_send()
 
     @pl.when(me_z != me_d)
     def _():
@@ -479,32 +507,39 @@
             pltpu.VMEM((dp, 8, sq_width), F32),
             pltpu.VMEM((dp, 8, sq_width), F32),
             pltpu.VMEM((dp, rows_d, width), BF16),
-            pltpu.VMEM((tp, rows_t, 2 * feats), BF16),
+            pltpu.VMEM((dp, per, rows_t, 2 * feats), F32),
+            pltpu.VMEM((dp, per, rows_t, 2 * feats), BF16),
+            pltpu.VMEM((dp, per, rows_t, 2 * feats), BF16),
+            pltpu.VMEM((dp, rows_t, 2 * feats), BF16),
             pltpu.VMEM((rows_t, 2 * feats), F32),
-            pltpu.VMEM((tp, rows_t, 2 * feats), BF16),
+            pltpu.VMEM((dp, rows_t, 2 * feats), BF16),
             pltpu.VMEM((dp, rows_t, feats), F32),
-            pltpu.VMEM((dp, 3, width, feats), BF16),
-            pltpu.VMEM((dp, 3, width, feats), BF16),
+            pltpu.VMEM((dp, width, feats), BF16),
+            pltpu.VMEM((dp, 2, width, feats), BF16),
+            pltpu.VMEM((dp, width, feats), BF16),
             pltpu.VMEM((dp, per, rows_t, feats), BF16),
             pltpu.VMEM((rows_d + width, 128), F32),
             pltpu.VMEM((rows_d + width, 128), F32),
             pltpu.VMEM((rows_d, 128), F32),
             pltpu.VMEM((rows_d, 128), F32),
-            pltpu.VMEM((dp, per, rows_t, 2 * feats), BF16),
-            pltpu.VMEM((dp, per, rows_t, 2 * feats), BF16),
+            pltpu.VMEM((dp, rows_d, width), BF16),
+            pltpu.VMEM((per, rows_t, 2 * feats), BF16),
+            pltpu.VMEM((per, rows_t, 2 * feats), BF16),
             dma(6), dma(layers, 8),
             dma(tp), dma(tp),
             dma(dp), dma(dp),
             dma(dp), dma(dp),
             dma(dp), dma(dp),
-            dma(tp), dma(tp),
-            dma(dp), dma(dp),
-            dma(2, 4), dma(2, 4),
-            dma(2, dp), dma(2, dp),
+            dma(dp, per), dma(dp, per),
+            dma(dp), dma(dp),
+            dma(dp), dma(dp),
+            dma(2, 2, 4), dma(2, 2, 4),
+            dma(dp), dma(dp),
             dma(dp, per), dma(dp, per),
             pltpu.SemaphoreType.DMA, pltpu.SemaphoreType.DMA,
             pltpu.SemaphoreType.DMA, pltpu.SemaphoreType.DMA,
-            dma(dp, per), dma(dp, per),
+            dma(dp), dma(dp),
+            dma(per), dma(per),
         ],
         compiler_params=pltpu.CompilerParams(collective_id=0, has_side_effects=True, vmem_limit_bytes=limit),
     )(

time: 55.5 us -> 53.6 us (0.966)
  the two profiles are of different devices: /device:TPU:1 before, /device:TPU:32 now
where the time goes in v3:
time: 53.6 us
  Pallas kernels  51.7 us (96%)
  local copies, waits for them, and re-layouts  1.25 us (2%)
  between operations  0.64 us (1%)
    pallas_call x1, Pallas kernels, per_device(): pl.pallas_call(functools.partial(kernel, tp, dp, chans), out_shape=(pltpu...  51.7 us
    unnamed x2, local copies, waits for them, and re-layouts  1.25 us

profile of v3, /device:TPU:32, one launch (start us, length us, event | category | flops | bytes accessed | tf_op | source)
XLA Modules:
  0.0 53.6 jit_solution(12252812180121108338)
XLA Ops:
  0.6 51.7 %shard_map.149 = (bf16[8,256]{1,0:T(8,128)(2,1)S(1)}, f32[2,128,128]{2,1,0:T(8,128)S(1)}) custom-call(bf16[8,256]{1,0:T(8,128)(2,1)} %stream_hbm.1, f32[2,256]{1,0:T(2,128)} %gain_hbm.1, bf16[2,64,256]{2,1,0:T(8,128)(2,1)} %bitcast.7, f32[2,4,64]{2,1,0:T(4,128)} %lam_re_hbm.1, f32[2,4,64]{2,1,0:T(4,128)} %lam_im_hbm.1, f32[2,4]{1,0:T(2,128)} %log_dt_hbm.1, ...), custom_call_target="tpu_custom_call" | custom-call | tf_op jit(solution)/shard_map/pallas_call | solution.py:479
  52.3 0.6 %copy.18 = bf16[8,256]{1,0:T(8,128)(2,1)} copy(bf16[8,256]{1,0:T(8,128)(2,1)S(1)} %get-tuple-element.6) | data formatting | bytes 8192
  52.9 0.7 %copy.19 = f32[2,32,4,128]{3,2,1,0:T(4,128)} copy(f32[2,32,4,128]{3,2,1,0:T(4,128)S(1)} %bitcast.5) | data formatting | bytes 262144

commit v4 on v3

--- a/solution.py
+++ b/solution.py
@@ -34,9 +34,9 @@
     out_ref, state,
     stream_ref, gain_ref, lam_re_ref, lam_im_ref, log_dt_ref, skip_ref, own_w, b_re, b_im, c_re, c_im, drive, read,
     kept, proj, u_keep, masked, from_old, mix_w,
-    x_all, part_send, part_recv, sq_send, sq_recv, mix_all, near_own, near_send, near_recv, comb_send, comb_own, comb_recv,
+    x_all, near_in, mix_all, near_own, near_send, near_recv, comb_send, comb_own, comb_recv,
     gain_all, col_in, col_out, far_in, x_far, swap_send, swap_recv, u_send, u_recv, mix_far, out_send, out_recv,
-    small_sem, load_sem, x_ss, x_rs, part_ss, part_rs, sq_ss, sq_rs, mix_ss, mix_rs, near_ss, near_rs, comb_ss, comb_rs,
+    small_sem, load_sem, x_ss, x_rs, in_ss, in_rs, mix_ss, mix_rs, near_ss, near_rs, comb_ss, comb_rs,
     gain_ss, gain_rs, col_ss, col_rs, row_ss, row_rs, xf_ss, xf_rs, swap_ss, swap_rs, u_ss, u_rs, mf_ss, mf_rs, of_ss, of_rs,
 ):
     layers = w_in_hbm.shape[0]
@@ -46,7 +46,6 @@
     per = rows_d // rows_t
     groups, half = lam_re_ref.shape[1:]
     lanes = state.shape[2]
-    sq_width = sq_send.shape[2]
     me_z, me_y = me_t // per, me_t % per
 
     barrier = pltpu.get_barrier_semaphore()
@@ -54,17 +53,18 @@
     def greet(t, d):
         pl.semaphore_signal(barrier, inc=1, device_id={"tp": t, "dp": d}, device_id_type=pl.DeviceIdType.MESH)
 
+    @pl.when(me_z != me_d)
+    def _():
+        for k in range(dp):
+            for j in range(per):
+                greet(me_d * per + j, partner(me_d, k, dp))
+
     for k in range(1, dp):
-        greet(me_t, partner(me_d, k, dp))
-    for k in range(1, tp):
-        greet(partner(me_t, k, tp), me_d)
-    for j in range(1, per):
-        for k in range(1, dp):
-            greet(me_z * per + partner(me_y, j, per), partner(me_d, k, dp))
-
-    @pl.when(me_z != me_d)
-    def _():
-        greet(me_d * per + me_y, me_z)
+        greet(partner(me_z, k, dp) * per + me_y, me_d)
+    for k in range(dp):
+        for j in range(per):
+            if k or j:
+                greet(me_z * per + partner(me_y, j, per), partner(me_d, k, dp))
 
     smalls = []
     for i, (src, dst) in enumerate(
@@ -95,15 +95,11 @@
             device_id_type=pl.DeviceIdType.MESH,
         )
 
-    def x_copy(k):
-        to = partner(me_t, k, tp)
-        return send(stream_ref, x_all.at[me_t], x_ss.at[to], x_rs.at[me_t], to, me_d)
-
-    def part_copy(to):
-        return send(part_send.at[to], part_recv.at[me_d], part_ss.at[to], part_rs.at[me_d], me_t, to)
-
-    def sq_copy(to):
-        return send(sq_send.at[to], sq_recv.at[me_d], sq_ss.at[to], sq_rs.at[me_d], me_t, to)
+    def x_copy(t):
+        return send(stream_ref, x_all.at[me_d, me_y], x_ss.at[t], x_rs.at[me_d, me_y], t, me_z)
+
+    def in_copy(to):
+        return send(own_w.at[0], near_in.at[me_d], in_ss.at[to], in_rs.at[me_d], me_t, to)
 
     def mix_copy(to):
         return send(mix_all.at[me_d], mix_all.at[me_d], mix_ss.at[to], mix_rs.at[me_d], me_t, to)
@@ -164,7 +160,6 @@
         return send(ref, ref, rs, rs, 0, 0)
 
     lane_group = lax.broadcasted_iota(jnp.int32, (rows_d, width), 1) // chans
-    eye = lax.broadcasted_iota(jnp.int32, (rows_d, sq_width), 0) == lax.broadcasted_iota(jnp.int32, (rows_d, sq_width), 1)
     group_eye = lax.broadcasted_iota(jnp.int32, (groups, groups), 0) == lax.broadcasted_iota(jnp.int32, (groups, groups), 1)
     wide_0 = lax.broadcasted_iota(jnp.int32, (width, width), 0)
     wide_1 = lax.broadcasted_iota(jnp.int32, (width, width), 1)
@@ -211,71 +206,74 @@
         for g in range(groups):
             state[l, pl.ds(g, rows_d, stride=groups), :] = kept[l, pl.ds(g * rows_d, rows_d), :]
 
-    elsewhere = ((me_z - me_d) * (me_z - me_d) + dp * dp - 1) // (dp * dp)
-    pl.semaphore_wait(barrier, tp - 1 + dp - 1 + (per - 1) * (dp - 1) + elsewhere)
+    pl.semaphore_wait(barrier, per * dp - 1 + dp - 1 + (dp - 1) * per)
 
     smalls[0].wait()
     for k in reversed(range(1, tp)):
-        x_copy(k).start()
+        x_copy(partner(me_t, k, tp)).start()
+
+    @pl.when(me_z != me_d)
+    def _():
+        x_copy(me_t).start()
+
+    @pl.when(me_z == me_d)
+    def _():
+        x_all[me_d, me_y] = stream_ref[...]
+
     smalls[1].wait()
-    gain_all[me_d] = jnp.broadcast_to(gain_ref[1:2, :], (rows_t, feats))
+    for l in range(layers):
+        gain_all[me_d, l] = jnp.broadcast_to(gain_ref[l : l + 1, :], (rows_t, feats))
+    loads[0, 5].wait()
     for k in reversed(range(1, dp)):
         gain_copy(partner(me_d, k, dp)).start()
+        in_copy(partner(me_d, k, dp)).start()
     loads[1, 5].wait()
     col_start(0, 1)
-    x_all[me_t] = stream_ref[...]
     for small in smalls[2:]:
         small.wait()
     from_old[...], mix_w[...] = prepare(0)
 
-    loads[0, 5].wait()
-    gain = gain_ref[0:1, :]
-    own_part = own_sq = None
-    for k in reversed(range(dp)):
-        if k == 6:
+    acc = jnp.zeros((rows_d, width), F32)
+    squares = jnp.zeros((rows_d, feats), F32)
+    for k in reversed(PLANE_FAR_FIRST):
+        if k == 7:
             col_wait(0, 1)
             col_start(0, 2)
-        to = partner(me_d, k, dp)
+        by = partner(me_d, k, dp, True)
+        if k:
+            arrival(gain_all.at[by], gain_rs.at[by]).wait_recv()
+            arrival(near_in.at[by], in_rs.at[by]).wait_recv()
         for j in range(per):
-            t = to * per + j
-
-            @pl.when(t != me_t)
-            def _():
-                arrival(x_all.at[t], x_rs.at[t]).wait_recv()
-
-        x = x_all[pl.ds(to * per, per)].astype(F32).reshape(rows_d, feats)
-        column = jnp.sum(x * x, axis=1, keepdims=True)
-        squares = jnp.sum(jnp.where(eye, column, 0.0), axis=0, keepdims=True)
-        product = lax.dot_general((x * gain).astype(BF16), own_w[0], NT, preferred_element_type=F32)
-        if k:
-            sq_send[to] = jnp.broadcast_to(squares, (8, sq_width))
-            sq_copy(to).start()
-            part_send[to] = product.astype(BF16)
-            part_copy(to).start()
-        else:
-            own_part, own_sq = product, squares
-    loads[1, 6].wait()
-    loads[1, 7].wait()
-    col_start(1, 1)
-    for k in range(1, dp):
-        by = partner(me_d, k, dp, True)
-        arrival(sq_recv.at[by], sq_rs.at[by]).wait_recv()
-        own_sq = own_sq + sq_recv[by][0:1, :]
-        arrival(part_recv.at[by], part_rs.at[by]).wait_recv()
-        own_part = own_part + part_recv[by].astype(F32)
-        if k == 2:
-            col_wait(0, 2)
-            col_start(0, 3, 4)
-    square_total = jnp.sum(jnp.where(eye, own_sq, 0.0), axis=1, keepdims=True)
-    u = lax.rsqrt(square_total / (feats * dp) + EPS) * own_part
+            y = partner(me_y, j, per)
+            if k or j:
+                arrival(x_all.at[by, y], x_rs.at[by, y]).wait_recv()
+            else:
+
+                @pl.when(me_z != me_d)
+                def _():
+                    arrival(x_all.at[by, y], x_rs.at[by, y]).wait_recv()
+
+        weights = near_in.at[by] if k else own_w.at[0]
+        x = x_all[by].astype(F32)
+        normed = (x * gain_all[by, 0][None]).astype(BF16).reshape(rows_d, feats)
+        x = x.reshape(rows_d, feats)
+        squares = squares + x * x
+        acc = acc + lax.dot_general(normed, weights[...], NT, preferred_element_type=F32)
+    u = lax.rsqrt(jnp.sum(squares, axis=1, keepdims=True) / (feats * dp) + EPS) * acc
     u_keep[...] = u
     pre = from_old[...] + jnp.dot(u, mix_w[...], precision=HIGHEST, preferred_element_type=F32)
     mix_all[me_d] = jax.nn.gelu(pre).astype(BF16)
     for k in reversed(range(1, dp)):
         mix_copy(partner(me_d, k, dp)).start()
+    loads[1, 6].wait()
+    loads[1, 7].wait()
+    col_start(1, 1)
     loads[0, 6].wait()
     loads[0, 7].wait()
     for k in range(dp):
+        if k == 2:
+            col_wait(0, 2)
+            col_start(0, 3, 4)
         by = partner(me_d, k, dp, True)
         if k:
             arrival(mix_all.at[by], mix_rs.at[by]).wait_recv()
@@ -307,11 +305,10 @@
         def _():
             comb_own[...] = total
 
-    col_wait(0, 3, 4)
-    for k in reversed(range(1, dp)):
-        row_copy(partner(me_d, k, dp)).start()
     for k in range(4):
         gather_near(k)
+    col_wait(1, 1)
+    col_start(1, 2)
     update(0, u_keep[...])
     total, mixer = prepare(1)
     swap_send[:rows_d] = jnp.concatenate([total, total], axis=1)
@@ -328,31 +325,38 @@
     for k in range(4, dp):
         gather_near(k)
     for k in range(1, tp):
-        x_copy(k).wait_send()
+        x_copy(partner(me_t, k, tp)).wait_send()
+
+    @pl.when(me_z != me_d)
+    def _():
+        x_copy(me_t).wait_send()
+
     for k in range(1, dp):
         to = partner(me_d, k, dp)
-        part_copy(to).wait_send()
-        sq_copy(to).wait_send()
+        in_copy(to).wait_send()
         mix_copy(to).wait_send()
         gain_copy(to).wait_send()
     for side in range(2):
         for i in range(1, 5):
             col_copy(0, side, i).wait_send()
 
-    col_wait(1, 1)
-    col_start(1, 2)
+    col_wait(0, 3, 4)
+    for k in reversed(range(1, dp)):
+        row_copy(partner(me_d, k, dp)).start()
     combined = comb_own[...]
     for k in range(1, dp):
         by = partner(me_z, k, dp, True)
         arrival(comb_recv.at[by], comb_rs.at[by]).wait_recv()
         combined = combined + comb_recv[by].astype(F32)
-    fresh = (x_all[me_t].astype(F32) + combined[:, :feats] * jax.nn.sigmoid(combined[:, feats:])).astype(BF16)
+    fresh = (stream_ref[...].astype(F32) + combined[:, :feats] * jax.nn.sigmoid(combined[:, feats:])).astype(BF16)
 
     x_far[me_d, me_y] = fresh
     for k in PLANE_FAR_FIRST:
         for j in ROW_FAR_FIRST:
             if k or j:
                 xf_copy(partner(me_y, j, per), partner(me_d, k, dp)).start()
+    col_wait(1, 2)
+    col_start(1, 3, 4)
     for k in range(1, dp):
         comb_copy(partner(me_z, k, dp)).wait_send()
     for k in range(dp):
@@ -363,17 +367,10 @@
     def _():
         swap_copy().wait_send()
 
-    for k in range(1, dp):
-        by = partner(me_d, k, dp, True)
-        arrival(gain_all.at[by], gain_rs.at[by]).wait_recv()
-
     acc = jnp.zeros((rows_d, width), F32)
     squares = jnp.zeros((rows_d, feats), F32)
     for k in reversed(PLANE_FAR_FIRST):
         by = partner(me_d, k, dp, True)
-        if k == 3:
-            col_wait(1, 2)
-            col_start(1, 3, 4)
         if k:
             arrival(far_in.at[by], row_rs.at[by]).wait_recv()
         weights = far_in.at[by] if k else col_in.at[me_d]
@@ -382,7 +379,7 @@
                 y = partner(me_y, j, per)
                 arrival(x_far.at[by, y], xf_rs.at[by, y]).wait_recv()
         x = x_far[by].astype(F32)
-        normed = (x * gain_all[by][None]).astype(BF16).reshape(rows_d, feats)
+        normed = (x * gain_all[by, 1][None]).astype(BF16).reshape(rows_d, feats)
         x = x.reshape(rows_d, feats)
         squares = squares + x * x
         acc = acc + lax.dot_general(normed, weights[...], NT, preferred_element_type=F32)
@@ -474,7 +471,6 @@
     limit = 67043328 - 4 * layers * rows_d * groups * lanes - (256 << 10)
     vmem = pl.BlockSpec(memory_space=pltpu.VMEM)
     hbm = pl.BlockSpec(memory_space=pltpu.HBM)
-    sq_width = max(rows_d, 128)
     dma = lambda *shape: pltpu.SemaphoreType.DMA(shape)
     out, states = pl.pallas_call(
         functools.partial(kernel, tp, dp, chans),
@@ -501,11 +497,8 @@
             pltpu.VMEM((rows_d * groups, width), F32),
             pltpu.VMEM((rows_d, width), F32),
             pltpu.VMEM((width, width), F32),
-            pltpu.VMEM((tp, rows_t, feats), BF16),
-            pltpu.VMEM((dp, rows_d, width), BF16),
-            pltpu.VMEM((dp, rows_d, width), BF16),
-            pltpu.VMEM((dp, 8, sq_width), F32),
-            pltpu.VMEM((dp, 8, sq_width), F32),
+            pltpu.VMEM((dp, per, rows_t, feats), BF16),
+            pltpu.VMEM((dp, width, feats), BF16),
             pltpu.VMEM((dp, rows_d, width), BF16),
             pltpu.VMEM((dp, per, rows_t, 2 * feats), F32),
             pltpu.VMEM((dp, per, rows_t, 2 * feats), BF16),
@@ -513,7 +506,7 @@
             pltpu.VMEM((dp, rows_t, 2 * feats), BF16),
             pltpu.VMEM((rows_t, 2 * feats), F32),
             pltpu.VMEM((dp, rows_t, 2 * feats), BF16),
-            pltpu.VMEM((dp, rows_t, feats), F32),
+            pltpu.VMEM((dp, layers, rows_t, feats), F32),
             pltpu.VMEM((dp, width, feats), BF16),
             pltpu.VMEM((dp, 2, width, feats), BF16),
             pltpu.VMEM((dp, width, feats), BF16),
@@ -526,8 +519,7 @@
             pltpu.VMEM((per, rows_t, 2 * feats), BF16),
             pltpu.VMEM((per, rows_t, 2 * feats), BF16),
             dma(6), dma(layers, 8),
-            dma(tp), dma(tp),
-            dma(dp), dma(dp),
+            dma(tp), dma(dp, per),
             dma(dp), dma(dp),
             dma(dp), dma(dp),
             dma(dp, per), dma(dp, per),

time: 53.6 us -> 50.4 us (0.940)
  the two profiles are of different devices: /device:TPU:32 before, /device:TPU:1 now
where the time goes in v4:
time: 50.4 us; the launch traced here: 50.3 us
  Pallas kernels  48.4 us (96%)
  local copies, waits for them, and re-layouts  1.25 us (2%)
  between operations  0.64 us (1%)
    pallas_call x1, Pallas kernels, per_device(): pl.pallas_call(functools.partial(kernel, tp, dp, chans), out_shape=(pltpu...  48.4 us
    unnamed x2, local copies, waits for them, and re-layouts  1.25 us

profile of v4, /device:TPU:1, one launch (start us, length us, event | category | flops | bytes accessed | tf_op | source)
XLA Modules:
  0.0 50.3 jit_solution(3852365214016639374)
XLA Ops:
  0.6 48.4 %shard_map.149 = (bf16[8,256]{1,0:T(8,128)(2,1)S(1)}, f32[2,128,128]{2,1,0:T(8,128)S(1)}) custom-call(bf16[8,256]{1,0:T(8,128)(2,1)} %stream_hbm.1, f32[2,256]{1,0:T(2,128)} %gain_hbm.1, bf16[2,64,256]{2,1,0:T(8,128)(2,1)} %bitcast.7, f32[2,4,64]{2,1,0:T(4,128)} %lam_re_hbm.1, f32[2,4,64]{2,1,0:T(4,128)} %lam_im_hbm.1, f32[2,4]{1,0:T(2,128)} %log_dt_hbm.1, ...), custom_call_target="tpu_custom_call" | custom-call | tf_op jit(solution)/shard_map/pallas_call | solution.py:475
  49.0 0.6 %copy.18 = bf16[8,256]{1,0:T(8,128)(2,1)} copy(bf16[8,256]{1,0:T(8,128)(2,1)S(1)} %get-tuple-element.6) | data formatting | bytes 8192
  49.6 0.7 %copy.19 = f32[2,32,4,128]{3,2,1,0:T(4,128)} copy(f32[2,32,4,128]{3,2,1,0:T(4,128)S(1)} %bitcast.5) | data formatting | bytes 262144

commit v5 on v4

--- a/solution.py
+++ b/solution.py
@@ -37,7 +37,7 @@
     x_all, near_in, mix_all, near_own, near_send, near_recv, comb_send, comb_own, comb_recv,
     gain_all, col_in, col_out, far_in, x_far, swap_send, swap_recv, u_send, u_recv, mix_far, out_send, out_recv,
     small_sem, load_sem, x_ss, x_rs, in_ss, in_rs, mix_ss, mix_rs, near_ss, near_rs, comb_ss, comb_rs,
-    gain_ss, gain_rs, col_ss, col_rs, row_ss, row_rs, xf_ss, xf_rs, swap_ss, swap_rs, u_ss, u_rs, mf_ss, mf_rs, of_ss, of_rs,
+    gain_ss, gain_rs, col_ss, col_rs, row_ss, row_rs, xf_ss, xf_rs, swap_ss, swap_rs, u_ss, u_rs, mf_ss, of_ss, of_rs,
 ):
     layers = w_in_hbm.shape[0]
     me_t, me_d = lax.axis_index("tp"), lax.axis_index("dp")
@@ -76,18 +76,16 @@
         smalls.append(pltpu.make_async_copy(src, dst, small_sem.at[i]))
         smalls[i].start()
     loads = {}
-    for l in range(layers):
-        weights = (
-            [own_w.at[i] for i in range(3)] if l == 0 else [col_in.at[me_z], col_out.at[me_z, 0], col_out.at[me_z, 1]]
+    for i, (src, dst) in enumerate(
+        (
+            (w_in_hbm.at[0], own_w.at[0]), (w_in_hbm.at[1], col_in.at[me_z]), (b_re_hbm, b_re), (b_im_hbm, b_im),
+            (c_re_hbm, c_re), (c_im_hbm, c_im), (state_hbm, state), (w_val_hbm.at[0], own_w.at[1]),
+            (w_gate_hbm.at[0], own_w.at[2]), (w_val_hbm.at[1], col_out.at[me_z, 0]),
+            (w_gate_hbm.at[1], col_out.at[me_z, 1]),
         )
-        for i, (src, dst) in enumerate(
-            (
-                (b_re_hbm, b_re.at[l]), (b_im_hbm, b_im.at[l]), (c_re_hbm, c_re.at[l]), (c_im_hbm, c_im.at[l]),
-                (state_hbm, state.at[l]), (w_in_hbm, weights[0]), (w_val_hbm, weights[1]), (w_gate_hbm, weights[2]),
-            )
-        ):
-            loads[l, i] = pltpu.make_async_copy(src.at[l], dst, load_sem.at[l, i])
-            loads[l, i].start()
+    ):
+        loads[i] = pltpu.make_async_copy(src, dst, load_sem.at[i])
+        loads[i].start()
 
     def send(src, dst, ss, rs, t, d):
         return pltpu.make_async_remote_copy(
@@ -96,24 +94,24 @@
         )
 
     def x_copy(t):
-        return send(stream_ref, x_all.at[me_d, me_y], x_ss.at[t], x_rs.at[me_d, me_y], t, me_z)
+        return send(stream_ref, x_all.at[me_d * per + me_y], x_ss, x_rs.at[me_d], t, me_z)
 
     def in_copy(to):
-        return send(own_w.at[0], near_in.at[me_d], in_ss.at[to], in_rs.at[me_d], me_t, to)
+        return send(own_w.at[0], near_in.at[me_d], in_ss, in_rs, me_t, to)
 
     def mix_copy(to):
-        return send(mix_all.at[me_d], mix_all.at[me_d], mix_ss.at[to], mix_rs.at[me_d], me_t, to)
+        return send(mix_all.at[me_d], mix_all.at[me_d], mix_ss, mix_rs.at[me_d], me_t, to)
 
     def near_copy(z, y):
         return send(
-            near_send.at[z, y], near_recv.at[z, me_y], near_ss.at[z, y], near_rs.at[z, me_y], me_z * per + y, me_d
+            near_send.at[z, y], near_recv.at[z, me_y], near_ss, near_rs.at[z], me_z * per + y, me_d
         )
 
     def comb_copy(z):
-        return send(comb_send.at[z], comb_recv.at[me_z], comb_ss.at[z], comb_rs.at[me_z], z * per + me_y, me_d)
+        return send(comb_send.at[z], comb_recv.at[me_z], comb_ss, comb_rs, z * per + me_y, me_d)
 
     def gain_copy(to):
-        return send(gain_all.at[me_d], gain_all.at[me_d], gain_ss.at[to], gain_rs.at[me_d], me_t, to)
+        return send(gain_all.at[me_d], gain_all.at[me_d], gain_ss, gain_rs, me_t, to)
 
     def col_part(what, home, side, i):
         if what:
@@ -125,30 +123,29 @@
         home = lax.rem(me_z - sign * min(i - 1, 2) + 2 * dp, dp)
         to = lax.rem(me_z + sign * (2 if i == 4 else 1) + dp, dp)
         part = col_part(what, home, side, i)
-        return send(part, part, col_ss.at[what, side, i - 1], col_rs.at[what, side, i - 1], to * per + me_y, me_d)
+        return send(part, part, col_ss.at[what], col_rs.at[what, min(i, 3) - 1], to * per + me_y, me_d)
 
     def col_start(what, *hops):
         for i in hops:
             for side in range(2):
                 col_copy(what, side, i).start()
 
-    def col_wait(what, *hops):
-        for i in hops:
-            for side in range(2):
-                home = lax.rem(me_z - (1 - 2 * side) * i + 2 * dp, dp)
-                arrival(col_part(what, home, side, i), col_rs.at[what, side, i - 1]).wait_recv()
+    def col_wait(what, hop):
+        blocks = pl.ds(0, 3 if hop == 3 else 2)
+        arrival((col_out if what else col_in).at[blocks], col_rs.at[what, hop - 1]).wait_recv()
 
     def row_copy(z):
-        return send(col_in.at[z], far_in.at[me_d], row_ss.at[z], row_rs.at[me_d], me_t, z)
+        return send(col_in.at[z], far_in.at[me_d], row_ss, row_rs, me_t, z)
 
     def mf_copy(to):
-        return send(mix_far.at[me_d], mix_far.at[me_d], mf_ss.at[to], mf_rs.at[me_d], me_t, to)
+        return send(mix_far.at[me_d], mix_far.at[me_d], mf_ss, mix_rs.at[me_d], me_t, to)
 
     def xf_copy(y, d):
-        return send(x_far.at[me_d, me_y], x_far.at[me_d, me_y], xf_ss.at[d, y], xf_rs.at[me_d, me_y], me_z * per + y, d)
+        mine = x_far.at[me_d * per + me_y]
+        return send(mine, mine, xf_ss, xf_rs.at[me_d], me_z * per + y, d)
 
     def of_copy(y):
-        return send(out_send.at[y], out_recv.at[me_y], of_ss.at[y], of_rs.at[me_y], me_z * per + y, me_d)
+        return send(out_send.at[y], out_recv.at[me_y], of_ss, of_rs, me_z * per + y, me_d)
 
     def swap_copy():
         return send(swap_send, swap_recv, swap_ss, swap_rs, me_d * per + me_y, me_z)
@@ -158,6 +155,9 @@
 
     def arrival(ref, rs):
         return send(ref, ref, rs, rs, 0, 0)
+
+    def sent(ref, ss):
+        send(ref, ref, ss, ss, 0, 0).wait_send()
 
     lane_group = lax.broadcasted_iota(jnp.int32, (rows_d, width), 1) // chans
     group_eye = lax.broadcasted_iota(jnp.int32, (groups, groups), 0) == lax.broadcasted_iota(jnp.int32, (groups, groups), 1)
@@ -176,8 +176,9 @@
         ratio_im = (keep_im * lam_re - (keep_re - 1.0) * lam_im) / denom
         keep_a = jnp.concatenate([keep_re, keep_re], axis=1)
         keep_b = jnp.concatenate([-keep_im, keep_im], axis=1)
-        for i in range(5):
-            loads[l, i].wait()
+        if l == 0:
+            for i in range(2, 7):
+                loads[i].wait()
         for g in range(groups):
             t_re, t_im = b_re[l, g], b_im[l, g]
             r_re, r_im = ratio_re[g : g + 1, :], ratio_im[g : g + 1, :]
@@ -218,16 +219,16 @@
 
     @pl.when(me_z == me_d)
     def _():
-        x_all[me_d, me_y] = stream_ref[...]
+        x_all[me_d * per + me_y] = stream_ref[...]
 
     smalls[1].wait()
     for l in range(layers):
         gain_all[me_d, l] = jnp.broadcast_to(gain_ref[l : l + 1, :], (rows_t, feats))
-    loads[0, 5].wait()
+    loads[0].wait()
     for k in reversed(range(1, dp)):
         gain_copy(partner(me_d, k, dp)).start()
         in_copy(partner(me_d, k, dp)).start()
-    loads[1, 5].wait()
+    loads[1].wait()
     col_start(0, 1)
     for small in smalls[2:]:
         small.wait()
@@ -241,20 +242,21 @@
             col_start(0, 2)
         by = partner(me_d, k, dp, True)
         if k:
-            arrival(gain_all.at[by], gain_rs.at[by]).wait_recv()
-            arrival(near_in.at[by], in_rs.at[by]).wait_recv()
-        for j in range(per):
-            y = partner(me_y, j, per)
-            if k or j:
-                arrival(x_all.at[by, y], x_rs.at[by, y]).wait_recv()
-            else:
-
-                @pl.when(me_z != me_d)
-                def _():
-                    arrival(x_all.at[by, y], x_rs.at[by, y]).wait_recv()
-
+            arrival(x_all.at[pl.ds(0, per)], x_rs.at[by]).wait_recv()
+        else:
+
+            @pl.when(me_z != me_d)
+            def _():
+                arrival(x_all.at[pl.ds(0, per)], x_rs.at[by]).wait_recv()
+
+            @pl.when(me_z == me_d)
+            def _():
+                arrival(x_all.at[pl.ds(0, per - 1)], x_rs.at[by]).wait_recv()
+
+            arrival(gain_all.at[pl.ds(0, dp - 1)], gain_rs).wait_recv()
+            arrival(near_in.at[pl.ds(0, dp - 1)], in_rs).wait_recv()
         weights = near_in.at[by] if k else own_w.at[0]
-        x = x_all[by].astype(F32)
+        x = x_all[pl.ds(by * per, per)].astype(F32)
         normed = (x * gain_all[by, 0][None]).astype(BF16).reshape(rows_d, feats)
         x = x.reshape(rows_d, feats)
         squares = squares + x * x
@@ -265,11 +267,11 @@
     mix_all[me_d] = jax.nn.gelu(pre).astype(BF16)
     for k in reversed(range(1, dp)):
         mix_copy(partner(me_d, k, dp)).start()
-    loads[1, 6].wait()
-    loads[1, 7].wait()
+    loads[9].wait()
+    loads[10].wait()
     col_start(1, 1)
-    loads[0, 6].wait()
-    loads[0, 7].wait()
+    loads[7].wait()
+    loads[8].wait()
     for k in range(dp):
         if k == 2:
             col_wait(0, 2)
@@ -291,10 +293,9 @@
     def gather_near(k):
         z = partner(me_d, k, dp, True)
         total = near_own[z, me_y]
+        arrival(near_recv.at[z, pl.ds(0, per - 1)], near_rs.at[z]).wait_recv()
         for j in range(1, per):
-            y = partner(me_y, j, per)
-            arrival(near_recv.at[z, y], near_rs.at[z, y]).wait_recv()
-            total = total + near_recv[z, y].astype(F32)
+            total = total + near_recv[z, partner(me_y, j, per)].astype(F32)
 
         @pl.when(z != me_z)
         def _():
@@ -324,44 +325,36 @@
 
     for k in range(4, dp):
         gather_near(k)
-    for k in range(1, tp):
-        x_copy(partner(me_t, k, tp)).wait_send()
-
-    @pl.when(me_z != me_d)
-    def _():
-        x_copy(me_t).wait_send()
-
-    for k in range(1, dp):
-        to = partner(me_d, k, dp)
-        in_copy(to).wait_send()
-        mix_copy(to).wait_send()
-        gain_copy(to).wait_send()
-    for side in range(2):
-        for i in range(1, 5):
-            col_copy(0, side, i).wait_send()
-
-    col_wait(0, 3, 4)
+    @pl.when(me_z != me_d)
+    def _():
+        sent(x_all, x_ss)
+
+    @pl.when(me_z == me_d)
+    def _():
+        sent(x_all.at[pl.ds(0, tp - 1)], x_ss)
+
+    sent(near_in.at[pl.ds(0, dp - 1)], in_ss)
+    sent(mix_all.at[pl.ds(0, dp - 1)], mix_ss)
+    sent(gain_all.at[pl.ds(0, dp - 1)], gain_ss)
+    sent(col_in.at[pl.ds(0, 7)], col_ss.at[0])
+    col_wait(0, 3)
     for k in reversed(range(1, dp)):
         row_copy(partner(me_d, k, dp)).start()
     combined = comb_own[...]
+    arrival(comb_recv.at[pl.ds(0, dp - 1)], comb_rs).wait_recv()
     for k in range(1, dp):
-        by = partner(me_z, k, dp, True)
-        arrival(comb_recv.at[by], comb_rs.at[by]).wait_recv()
-        combined = combined + comb_recv[by].astype(F32)
+        combined = combined + comb_recv[partner(me_z, k, dp)].astype(F32)
     fresh = (stream_ref[...].astype(F32) + combined[:, :feats] * jax.nn.sigmoid(combined[:, feats:])).astype(BF16)
 
-    x_far[me_d, me_y] = fresh
+    x_far[me_d * per + me_y] = fresh
     for k in PLANE_FAR_FIRST:
         for j in ROW_FAR_FIRST:
             if k or j:
                 xf_copy(partner(me_y, j, per), partner(me_d, k, dp)).start()
     col_wait(1, 2)
     col_start(1, 3, 4)
-    for k in range(1, dp):
-        comb_copy(partner(me_z, k, dp)).wait_send()
-    for k in range(dp):
-        for j in range(1, per):
-            near_copy(k, partner(me_y, j, per)).wait_send()
+    sent(comb_send.at[pl.ds(0, dp - 1)], comb_ss)
+    sent(near_send.at[:, pl.ds(0, per - 1)], near_ss)
 
     @pl.when(me_z != me_d)
     def _():
@@ -371,14 +364,11 @@
     squares = jnp.zeros((rows_d, feats), F32)
     for k in reversed(PLANE_FAR_FIRST):
         by = partner(me_d, k, dp, True)
-        if k:
-            arrival(far_in.at[by], row_rs.at[by]).wait_recv()
+        arrival(x_far.at[pl.ds(0, per if k else per - 1)], xf_rs.at[by]).wait_recv()
+        if k == 1:
+            arrival(far_in.at[pl.ds(0, dp - 1)], row_rs).wait_recv()
         weights = far_in.at[by] if k else col_in.at[me_d]
-        for j in reversed(ROW_FAR_FIRST):
-            if k or j:
-                y = partner(me_y, j, per)
-                arrival(x_far.at[by, y], xf_rs.at[by, y]).wait_recv()
-        x = x_far[by].astype(F32)
+        x = x_far[pl.ds(by * per, per)].astype(F32)
         normed = (x * gain_all[by, 1][None]).astype(BF16).reshape(rows_d, feats)
         x = x.reshape(rows_d, feats)
         squares = squares + x * x
@@ -402,22 +392,16 @@
     for k in PLANE_FAR_FIRST:
         if k:
             mf_copy(partner(me_d, k, dp)).start()
-    col_wait(1, 3, 4)
-    for k in range(dp):
-        for j in range(per):
-            if k or j:
-                xf_copy(partner(me_y, j, per), partner(me_d, k, dp)).wait_send()
-    for k in range(1, dp):
-        row_copy(partner(me_d, k, dp)).wait_send()
-    for side in range(2):
-        for i in range(1, 5):
-            col_copy(1, side, i).wait_send()
+    col_wait(1, 3)
+    sent(x_far.at[pl.ds(0, tp - 1)], xf_ss)
+    sent(far_in.at[pl.ds(0, dp - 1)], row_ss)
+    sent(col_out.at[pl.ds(0, 7)], col_ss.at[1])
     value = jnp.zeros((rows_d, feats), F32)
     gate = jnp.zeros((rows_d, feats), F32)
     for k in reversed(PLANE_FAR_FIRST):
         by = partner(me_d, k, dp, True)
         if k:
-            arrival(mix_far.at[by], mf_rs.at[by]).wait_recv()
+            arrival(mix_far.at[by], mix_rs.at[by]).wait_recv()
         mixed = mix_far[by]
         value = value + jnp.dot(mixed, col_out[by, 0], preferred_element_type=F32)
         gate = gate + jnp.dot(mixed, col_out[by, 1], preferred_element_type=F32)
@@ -435,19 +419,15 @@
 
     update(1, u_recv[:, :width])
     combined = near_own[0, me_y]
-    for j in reversed(ROW_FAR_FIRST):
-        if j:
-            y = partner(me_y, j, per)
-            arrival(out_recv.at[y], of_rs.at[y]).wait_recv()
-            combined = combined + out_recv[y].astype(F32)
+    arrival(out_recv.at[pl.ds(0, per - 1)], of_rs).wait_recv()
+    for j in range(1, per):
+        combined = combined + out_recv[partner(me_y, j, per)].astype(F32)
     out_ref[...] = (
-        x_far[me_d, me_y].astype(F32) + combined[:, :feats] * jax.nn.sigmoid(combined[:, feats:])
+        x_far[me_d * per + me_y].astype(F32) + combined[:, :feats] * jax.nn.sigmoid(combined[:, feats:])
     ).astype(BF16)
 
-    for k in range(1, dp):
-        mf_copy(partner(me_d, k, dp)).wait_send()
-    for j in range(1, per):
-        of_copy(partner(me_y, j, per)).wait_send()
+    sent(mix_far.at[pl.ds(0, dp - 1)], mf_ss)
+    sent(out_send.at[pl.ds(0, per - 1)], of_ss)
 
     @pl.when(me_z != me_d)
     def _():
@@ -471,7 +451,8 @@
     limit = 67043328 - 4 * layers * rows_d * groups * lanes - (256 << 10)
     vmem = pl.BlockSpec(memory_space=pltpu.VMEM)
     hbm = pl.BlockSpec(memory_space=pltpu.HBM)
-    dma = lambda *shape: pltpu.SemaphoreType.DMA(shape)
+    one = pltpu.SemaphoreType.DMA
+    dma = lambda *shape: one(shape)
     out, states = pl.pallas_call(
         functools.partial(kernel, tp, dp, chans),
         out_shape=(pltpu.VMEM(stream.shape, BF16), pltpu.VMEM((layers, rows_d * groups, lanes), F32)),
@@ -497,7 +478,7 @@
             pltpu.VMEM((rows_d * groups, width), F32),
             pltpu.VMEM((rows_d, width), F32),
             pltpu.VMEM((width, width), F32),
-            pltpu.VMEM((dp, per, rows_t, feats), BF16),
+            pltpu.VMEM((tp, rows_t, feats), BF16),
             pltpu.VMEM((dp, width, feats), BF16),
             pltpu.VMEM((dp, rows_d, width), BF16),
             pltpu.VMEM((dp, per, rows_t, 2 * feats), F32),
@@ -510,7 +491,7 @@
             pltpu.VMEM((dp, width, feats), BF16),
             pltpu.VMEM((dp, 2, width, feats), BF16),
             pltpu.VMEM((dp, width, feats), BF16),
-            pltpu.VMEM((dp, per, rows_t, feats), BF16),
+            pltpu.VMEM((tp, rows_t, feats), BF16),
             pltpu.VMEM((rows_d + width, 128), F32),
             pltpu.VMEM((rows_d + width, 128), F32),
             pltpu.VMEM((rows_d, 128), F32),
@@ -518,20 +499,19 @@
             pltpu.VMEM((dp, rows_d, width), BF16),
             pltpu.VMEM((per, rows_t, 2 * feats), BF16),
             pltpu.VMEM((per, rows_t, 2 * feats), BF16),
-            dma(6), dma(layers, 8),
-            dma(tp), dma(dp, per),
-            dma(dp), dma(dp),
-            dma(dp), dma(dp),
-            dma(dp, per), dma(dp, per),
-            dma(dp), dma(dp),
-            dma(dp), dma(dp),
-            dma(2, 2, 4), dma(2, 2, 4),
-            dma(dp), dma(dp),
-            dma(dp, per), dma(dp, per),
-            pltpu.SemaphoreType.DMA, pltpu.SemaphoreType.DMA,
-            pltpu.SemaphoreType.DMA, pltpu.SemaphoreType.DMA,
-            dma(dp), dma(dp),
-            dma(per), dma(per),
+            dma(6), dma(11),
+            one, dma(dp),
+            one, one,
+            one, dma(dp),
+            one, dma(dp),
+            one, one,
+            one, one,
+            dma(2), dma(2, 3),
+            one, one,
+            one, dma(dp),
+            one, one,
+            one, one,
+            one, one, one,
         ],
         compiler_params=pltpu.CompilerParams(collective_id=0, has_side_effects=True, vmem_limit_bytes=limit),
     )(

time: 50.4 us -> 47.9 us (0.950)
  Pallas kernels: 48.4 us -> 45.9 us
    pallas_call x1, Pallas kernels: 48.4 us -> 45.9 us  [per_device(): pl.pallas_call(functools.partial(kernel, tp, dp, chans), out_shape=(pltpu...]
where the time goes in v5:
time: 47.9 us; the launch traced here: 47.8 us
  Pallas kernels  45.9 us (96%)
  local copies, waits for them, and re-layouts  1.25 us (3%)
  between operations  0.64 us (1%)
    pallas_call x1, Pallas kernels, per_device(): pl.pallas_call(functools.partial(kernel, tp, dp, chans), out_shape=(pltpu...  45.9 us
    unnamed x2, local copies, waits for them, and re-layouts  1.25 us

profile of v5, /device:TPU:1, one launch (start us, length us, event | category | flops | bytes accessed | tf_op | source)
XLA Modules:
  0.0 47.8 jit_solution(7268928805012751690)
XLA Ops:
  0.6 45.9 %shard_map.149 = (bf16[8,256]{1,0:T(8,128)(2,1)S(1)}, f32[2,128,128]{2,1,0:T(8,128)S(1)}) custom-call(bf16[8,256]{1,0:T(8,128)(2,1)} %stream_hbm.1, f32[2,256]{1,0:T(2,128)} %gain_hbm.1, bf16[2,64,256]{2,1,0:T(8,128)(2,1)} %bitcast.7, f32[2,4,64]{2,1,0:T(4,128)} %lam_re_hbm.1, f32[2,4,64]{2,1,0:T(4,128)} %lam_im_hbm.1, f32[2,4]{1,0:T(2,128)} %log_dt_hbm.1, ...), custom_call_target="tpu_custom_call" | custom-call | tf_op jit(solution)/shard_map/pallas_call | solution.py:456
  46.5 0.6 %copy.18 = bf16[8,256]{1,0:T(8,128)(2,1)} copy(bf16[8,256]{1,0:T(8,128)(2,1)S(1)} %get-tuple-element.6) | data formatting | bytes 8192
  47.1 0.7 %copy.19 = f32[2,32,4,128]{3,2,1,0:T(4,128)} copy(f32[2,32,4,128]{3,2,1,0:T(4,128)S(1)} %bitcast.5) | data formatting | bytes 262144

commit v6 on v5

--- a/solution.py
+++ b/solution.py
@@ -25,6 +25,11 @@
         found = found + (bit * (1 - mine) if k & bit else bit * mine)
         bit *= 2
     return found
+
+
+def ring_far_first(n, m):
+    others = [(a, b) for a in range(n) for b in range(m) if a or b]
+    return sorted(others, key=lambda o: -min(o[0], n - o[0]) - min(o[1], m - o[1]))
 
 
 def kernel(
@@ -210,8 +215,8 @@
     pl.semaphore_wait(barrier, per * dp - 1 + dp - 1 + (dp - 1) * per)
 
     smalls[0].wait()
-    for k in reversed(range(1, tp)):
-        x_copy(partner(me_t, k, tp)).start()
+    for a, b in ring_far_first(dp, per):
+        x_copy(lax.rem(me_z + a, dp) * per + lax.rem(me_y + b, per)).start()
 
     @pl.when(me_z != me_d)
     def _():
@@ -225,9 +230,10 @@
     for l in range(layers):
         gain_all[me_d, l] = jnp.broadcast_to(gain_ref[l : l + 1, :], (rows_t, feats))
     loads[0].wait()
-    for k in reversed(range(1, dp)):
-        gain_copy(partner(me_d, k, dp)).start()
-        in_copy(partner(me_d, k, dp)).start()
+    for k in PLANE_FAR_FIRST:
+        if k:
+            gain_copy(partner(me_d, k, dp)).start()
+            in_copy(partner(me_d, k, dp)).start()
     loads[1].wait()
     col_start(0, 1)
     for small in smalls[2:]:
@@ -265,15 +271,16 @@
     u_keep[...] = u
     pre = from_old[...] + jnp.dot(u, mix_w[...], precision=HIGHEST, preferred_element_type=F32)
     mix_all[me_d] = jax.nn.gelu(pre).astype(BF16)
-    for k in reversed(range(1, dp)):
-        mix_copy(partner(me_d, k, dp)).start()
+    for k in PLANE_FAR_FIRST:
+        if k:
+            mix_copy(partner(me_d, k, dp)).start()
     loads[9].wait()
     loads[10].wait()
     col_start(1, 1)
     loads[7].wait()
     loads[8].wait()
-    for k in range(dp):
-        if k == 2:
+    for k in reversed(PLANE_FAR_FIRST):
+        if k == 3:
             col_wait(0, 2)
             col_start(0, 3, 4)
         by = partner(me_d, k, dp, True)
@@ -306,10 +313,8 @@
         def _():
             comb_own[...] = total
 
-    for k in range(4):
-        gather_near(k)
-    col_wait(1, 1)
-    col_start(1, 2)
+    gather_near(0)
+    gather_near(1)
     update(0, u_keep[...])
     total, mixer = prepare(1)
     swap_send[:rows_d] = jnp.concatenate([total, total], axis=1)
@@ -323,8 +328,10 @@
     def _():
         swap_recv[...] = swap_send[...]
 
-    for k in range(4, dp):
+    for k in reversed(PLANE_FAR_FIRST[:6]):
         gather_near(k)
+    col_wait(1, 1)
+    col_start(1, 2)
     @pl.when(me_z != me_d)
     def _():
         sent(x_all, x_ss)
@@ -432,6 +439,17 @@
     @pl.when(me_z != me_d)
     def _():
         u_copy().wait_send()
+
+
+def put(out_ref, states_ref, out_hbm, states_hbm, sems):
+    copies = [
+        pltpu.make_async_copy(states_ref, states_hbm, sems.at[0]),
+        pltpu.make_async_copy(out_ref, out_hbm, sems.at[1]),
+    ]
+    for copy in copies:
+        copy.start()
+    for copy in copies:
+        copy.wait()
 
 
 def per_device(
@@ -519,6 +537,14 @@
         readout_imaginary, d_skip, w_val, w_gate,
         state.reshape(layers, rows_d * groups, lanes),
     )
+    out, states = pl.pallas_call(
+        put,
+        out_shape=(jax.ShapeDtypeStruct(out.shape, BF16), jax.ShapeDtypeStruct(states.shape, F32)),
+        in_specs=[vmem, vmem],
+        out_specs=(hbm, hbm),
+        scratch_shapes=[dma(2)],
+        compiler_params=pltpu.CompilerParams(vmem_limit_bytes=1 << 20),
+    )(out, states)
     return out, states.reshape(state.shape)
 
 

time: 47.9 us -> 46.2 us (0.965)
  local copies, waits for them, and re-layouts: 1.25 us -> 0 us
    unnamed x2 -> x0, local copies, waits for them, and re-layouts: 1.25 us -> none
    pallas_call x1, Pallas kernels: 45.9 us -> 44.8 us  [per_device(): pl.pallas_call(functools.partial(kernel, tp, dp, chans), out_shape=(pltpu...]
    pallas_call x0 -> x1, Pallas kernels: none -> 0.68 us  [per_device(): pl.pallas_call(put, out_shape=(jax.ShapeDtypeStruct(out.shape, BF16), jax...]
where the time goes in v6:
time: 46.2 us; the launch traced here: 46.1 us
  Pallas kernels  45.5 us (98%)
  between operations  0.64 us (1%)
    pallas_call x1, Pallas kernels, per_device(): pl.pallas_call(functools.partial(kernel, tp, dp, chans), out_shape=(pltpu...  44.8 us

profile of v6, /device:TPU:1, one launch (start us, length us, event | category | flops | bytes accessed | tf_op | source)
XLA Modules:
  0.0 46.1 jit_solution(13573986443417024510)
XLA Ops:
  0.6 44.8 %shard_map.149 = (bf16[8,256]{1,0:T(8,128)(2,1)S(1)}, f32[2,128,128]{2,1,0:T(8,128)S(1)}) custom-call(bf16[8,256]{1,0:T(8,128)(2,1)} %stream_hbm.1, f32[2,256]{1,0:T(2,128)} %gain_hbm.1, bf16[2,64,256]{2,1,0:T(8,128)(2,1)} %bitcast.6, f32[2,4,64]{2,1,0:T(4,128)} %lam_re_hbm.1, f32[2,4,64]{2,1,0:T(4,128)} %lam_im_hbm.1, f32[2,4]{1,0:T(2,128)} %log_dt_hbm.1, ...), custom_call_target="tpu_custom_call" | custom-call | tf_op jit(solution)/shard_map/pallas_call | solution.py:474
  45.4 0.7 %shard_map.150 = (bf16[8,256]{1,0:T(8,128)(2,1)}, f32[2,128,128]{2,1,0:T(8,128)}) custom-call(bf16[8,256]{1,0:T(8,128)(2,1)S(1)} %get-tuple-element.6.out_ref, f32[2,128,128]{2,1,0:T(8,128)S(1)} %get-tuple-element.7.states_ref), custom_call_target="tpu_custom_call" | custom-call | tf_op jit(solution)/shard_map/pallas_call | solution.py:540

commit v7 on v6

--- a/solution.py
+++ b/solution.py
@@ -39,10 +39,10 @@
     out_ref, state,
     stream_ref, gain_ref, lam_re_ref, lam_im_ref, log_dt_ref, skip_ref, own_w, b_re, b_im, c_re, c_im, drive, read,
     kept, proj, u_keep, masked, from_old, mix_w,
-    x_all, near_in, mix_all, near_own, near_send, near_recv, comb_send, comb_own, comb_recv,
-    gain_all, col_in, col_out, far_in, x_far, swap_send, swap_recv, u_send, u_recv, mix_far, out_send, out_recv,
-    small_sem, load_sem, x_ss, x_rs, in_ss, in_rs, mix_ss, mix_rs, near_ss, near_rs, comb_ss, comb_rs,
-    gain_ss, gain_rs, col_ss, col_rs, row_ss, row_rs, xf_ss, xf_rs, swap_ss, swap_rs, u_ss, u_rs, mf_ss, of_ss, of_rs,
+    x_all, x_old, near_in, mix_out, mix_all, near_recv, out_own,
+    gain_all, col_in, col_out, col_now, x_keep, part_send, part_recv, swap_send, swap_recv, u_send, u_recv, mix_far, out_send, out_recv,
+    small_sem, load_sem, x_ss, x_rs, old_ss, old_rs, in_ss, in_rs, mix_ss, mix_rs, near_ss, near_rs,
+    gain_ss, gain_rs, col_ss, col_rs, part_ss, part_rs, swap_ss, swap_rs, u_ss, u_rs, mf_ss, of_ss, of_rs,
 ):
     layers = w_in_hbm.shape[0]
     me_t, me_d = lax.axis_index("tp"), lax.axis_index("dp")
@@ -64,8 +64,8 @@
             for j in range(per):
                 greet(me_d * per + j, partner(me_d, k, dp))
 
-    for k in range(1, dp):
-        greet(partner(me_z, k, dp) * per + me_y, me_d)
+    for hop in (1, -1, 2, -2):
+        greet(lax.rem(me_z + hop + dp, dp) * per + me_y, me_d)
     for k in range(dp):
         for j in range(per):
             if k or j:
@@ -83,9 +83,9 @@
     loads = {}
     for i, (src, dst) in enumerate(
         (
-            (w_in_hbm.at[0], own_w.at[0]), (w_in_hbm.at[1], col_in.at[me_z]), (b_re_hbm, b_re), (b_im_hbm, b_im),
-            (c_re_hbm, c_re), (c_im_hbm, c_im), (state_hbm, state), (w_val_hbm.at[0], own_w.at[1]),
-            (w_gate_hbm.at[0], own_w.at[2]), (w_val_hbm.at[1], col_out.at[me_z, 0]),
+            (w_in_hbm.at[0], own_w), (w_in_hbm.at[1], col_in.at[me_z]), (b_re_hbm, b_re), (b_im_hbm, b_im),
+            (c_re_hbm, c_re), (c_im_hbm, c_im), (state_hbm, state), (w_val_hbm.at[0], col_now.at[me_z, 0]),
+            (w_gate_hbm.at[0], col_now.at[me_z, 1]), (w_val_hbm.at[1], col_out.at[me_z, 0]),
             (w_gate_hbm.at[1], col_out.at[me_z, 1]),
         )
     ):
@@ -102,26 +102,27 @@
         return send(stream_ref, x_all.at[me_d * per + me_y], x_ss, x_rs.at[me_d], t, me_z)
 
     def in_copy(to):
-        return send(own_w.at[0], near_in.at[me_d], in_ss, in_rs, me_t, to)
+        return send(own_w, near_in.at[me_d], in_ss, in_rs, me_t, to)
+
+    def old_copy(y):
+        return send(stream_ref, x_old.at[me_y], old_ss, old_rs, me_z * per + y, me_d)
 
     def mix_copy(to):
-        return send(mix_all.at[me_d], mix_all.at[me_d], mix_ss, mix_rs.at[me_d], me_t, to)
-
-    def near_copy(z, y):
-        return send(
-            near_send.at[z, y], near_recv.at[z, me_y], near_ss, near_rs.at[z], me_z * per + y, me_d
-        )
-
-    def comb_copy(z):
-        return send(comb_send.at[z], comb_recv.at[me_z], comb_ss, comb_rs, z * per + me_y, me_d)
+        return send(mix_out, mix_all.at[me_z], mix_ss, mix_rs.at[me_z], me_d * per + me_y, to)
+
+    def near_copy(y):
+        return send(near_recv.at[me_y], near_recv.at[me_y], near_ss, near_rs, me_z * per + y, me_d)
 
     def gain_copy(to):
         return send(gain_all.at[me_d], gain_all.at[me_d], gain_ss, gain_rs, me_t, to)
 
     def col_part(what, home, side, i):
-        if what:
-            return col_out.at[home, :, pl.ds(side * (width // 2), width // 2)] if i == 4 else col_out.at[home]
-        return col_in.at[home, pl.ds(side * (width // 2), width // 2)] if i == 4 else col_in.at[home]
+        rows = pl.ds(side * (width // 2), width // 2)
+        if what == 1:
+            held = col_out.at[home]
+            return held.at[:, rows] if i == 4 else held
+        held = col_now.at[home, what - 2] if what else col_in.at[home]
+        return held.at[rows] if i == 4 else held
 
     def col_copy(what, side, i):
         sign = 1 - 2 * side
@@ -137,18 +138,15 @@
 
     def col_wait(what, hop):
         blocks = pl.ds(0, 3 if hop == 3 else 2)
-        arrival((col_out if what else col_in).at[blocks], col_rs.at[what, hop - 1]).wait_recv()
-
-    def row_copy(z):
-        return send(col_in.at[z], far_in.at[me_d], row_ss, row_rs, me_t, z)
+        held = (col_in.at[blocks], col_out.at[blocks], col_now.at[blocks, 0], col_now.at[blocks, 1])[what]
+        arrival(held, col_rs.at[what, hop - 1]).wait_recv()
+
+    def part_copy(to):
+        return send(part_send.at[to], part_recv.at[me_d], part_ss, part_rs, me_t, to)
 
     def mf_copy(to):
         return send(mix_far.at[me_d], mix_far.at[me_d], mf_ss, mix_rs.at[me_d], me_t, to)
 
-    def xf_copy(y, d):
-        mine = x_far.at[me_d * per + me_y]
-        return send(mine, mine, xf_ss, xf_rs.at[me_d], me_z * per + y, d)
-
     def of_copy(y):
         return send(out_send.at[y], out_recv.at[me_y], of_ss, of_rs, me_z * per + y, me_d)
 
@@ -163,6 +161,9 @@
 
     def sent(ref, ss):
         send(ref, ref, ss, ss, 0, 0).wait_send()
+
+    def fold(tall):
+        return jnp.concatenate([tall[: rows_d // 2], tall[rows_d // 2 :]], axis=1)
 
     lane_group = lax.broadcasted_iota(jnp.int32, (rows_d, width), 1) // chans
     group_eye = lax.broadcasted_iota(jnp.int32, (groups, groups), 0) == lax.broadcasted_iota(jnp.int32, (groups, groups), 1)
@@ -212,7 +213,7 @@
         for g in range(groups):
             state[l, pl.ds(g, rows_d, stride=groups), :] = kept[l, pl.ds(g * rows_d, rows_d), :]
 
-    pl.semaphore_wait(barrier, per * dp - 1 + dp - 1 + (dp - 1) * per)
+    pl.semaphore_wait(barrier, per * dp - 1 + 4 + (dp - 1) * per)
 
     smalls[0].wait()
     for a, b in ring_far_first(dp, per):
@@ -227,25 +228,33 @@
         x_all[me_d * per + me_y] = stream_ref[...]
 
     smalls[1].wait()
-    for l in range(layers):
-        gain_all[me_d, l] = jnp.broadcast_to(gain_ref[l : l + 1, :], (rows_t, feats))
+    gain_all[me_d] = jnp.broadcast_to(gain_ref[0:1, :], (rows_t, feats))
     loads[0].wait()
     for k in PLANE_FAR_FIRST:
         if k:
             gain_copy(partner(me_d, k, dp)).start()
             in_copy(partner(me_d, k, dp)).start()
-    loads[1].wait()
-    col_start(0, 1)
+    x_old[me_y] = stream_ref[...]
+    for j in ROW_FAR_FIRST:
+        if j:
+            old_copy(partner(me_y, j, per)).start()
+    loads[7].wait()
+    loads[8].wait()
+    col_start(2, 1)
+    col_start(3, 1)
     for small in smalls[2:]:
         small.wait()
     from_old[...], mix_w[...] = prepare(0)
 
+    for what in (2, 3):
+        col_wait(what, 1)
+        col_start(what, 2)
+    loads[1].wait()
+    col_start(0, 1)
+
     acc = jnp.zeros((rows_d, width), F32)
     squares = jnp.zeros((rows_d, feats), F32)
     for k in reversed(PLANE_FAR_FIRST):
-        if k == 7:
-            col_wait(0, 1)
-            col_start(0, 2)
         by = partner(me_d, k, dp, True)
         if k:
             arrival(x_all.at[pl.ds(0, per)], x_rs.at[by]).wait_recv()
@@ -261,64 +270,77 @@
 
             arrival(gain_all.at[pl.ds(0, dp - 1)], gain_rs).wait_recv()
             arrival(near_in.at[pl.ds(0, dp - 1)], in_rs).wait_recv()
-        weights = near_in.at[by] if k else own_w.at[0]
+        weights = near_in.at[by] if k else own_w
         x = x_all[pl.ds(by * per, per)].astype(F32)
-        normed = (x * gain_all[by, 0][None]).astype(BF16).reshape(rows_d, feats)
+        normed = (x * gain_all[by][None]).astype(BF16).reshape(rows_d, feats)
         x = x.reshape(rows_d, feats)
         squares = squares + x * x
         acc = acc + lax.dot_general(normed, weights[...], NT, preferred_element_type=F32)
     u = lax.rsqrt(jnp.sum(squares, axis=1, keepdims=True) / (feats * dp) + EPS) * acc
     u_keep[...] = u
     pre = from_old[...] + jnp.dot(u, mix_w[...], precision=HIGHEST, preferred_element_type=F32)
-    mix_all[me_d] = jax.nn.gelu(pre).astype(BF16)
-    for k in PLANE_FAR_FIRST:
-        if k:
-            mix_copy(partner(me_d, k, dp)).start()
+    mix_out[...] = fold(jax.nn.gelu(pre).astype(BF16))
+    for k in PLANE_FAR_FIRST[:-1]:
+        mix_copy(partner(me_d, k, dp)).start()
+
+    @pl.when(me_z != me_d)
+    def _():
+        mix_copy(me_d).start()
+
+    @pl.when(me_z == me_d)
+    def _():
+        mix_all[me_z] = mix_out[...]
+
+    for what in (2, 3):
+        col_wait(what, 2)
+        col_start(what, 3, 4)
+    col_wait(0, 1)
+    col_start(0, 2)
     loads[9].wait()
     loads[10].wait()
     col_start(1, 1)
-    loads[7].wait()
-    loads[8].wait()
-    for k in reversed(PLANE_FAR_FIRST):
-        if k == 3:
+
+    def project(blocks, weights, arrive):
+        value = jnp.zeros((rows_d, feats), F32)
+        gate = jnp.zeros((rows_d, feats), F32)
+        for i, (block, held) in enumerate(blocks):
+            arrive(i, block)
+            mixed = held[block]
+            mixed = jnp.concatenate([mixed[:, :width], mixed[:, width:]], axis=0)
+            value = value + jnp.dot(mixed, weights[block, 0], preferred_element_type=F32)
+            gate = gate + jnp.dot(mixed, weights[block, 1], preferred_element_type=F32)
+        return value, gate
+
+    def arrive_now(i, block):
+        if i == 5:
+            col_wait(2, 3)
+            col_wait(3, 3)
             col_wait(0, 2)
             col_start(0, 3, 4)
-        by = partner(me_d, k, dp, True)
-        if k:
-            arrival(mix_all.at[by], mix_rs.at[by]).wait_recv()
-        mixed = mix_all[by]
-        value = jnp.dot(mixed, own_w[1], preferred_element_type=F32)
-        gate = jnp.dot(mixed, own_w[2], preferred_element_type=F32)
-        near_own[by, :, :, :feats] = value.reshape(per, rows_t, feats)
-        near_own[by, :, :, feats:] = gate.reshape(per, rows_t, feats)
-        near_send[by, :, :, :feats] = value.astype(BF16).reshape(per, rows_t, feats)
-        near_send[by, :, :, feats:] = gate.astype(BF16).reshape(per, rows_t, feats)
-        for j in ROW_FAR_FIRST:
-            if j:
-                near_copy(by, partner(me_y, j, per)).start()
-
-    def gather_near(k):
-        z = partner(me_d, k, dp, True)
-        total = near_own[z, me_y]
-        arrival(near_recv.at[z, pl.ds(0, per - 1)], near_rs.at[z]).wait_recv()
-        for j in range(1, per):
-            total = total + near_recv[z, partner(me_y, j, per)].astype(F32)
-
-        @pl.when(z != me_z)
-        def _():
-            comb_send[z] = total.astype(BF16)
-            comb_copy(z).start()
-
-        @pl.when(z == me_z)
-        def _():
-            comb_own[...] = total
-
-    gather_near(0)
-    gather_near(1)
+        if i:
+            arrival(mix_all.at[block], mix_rs.at[block]).wait_recv()
+        else:
+
+            @pl.when(me_z != me_d)
+            def _():
+                arrival(mix_all.at[block], mix_rs.at[block]).wait_recv()
+
+    nearest = [lax.rem(me_z + hop + dp, dp) for hop in (0, 1, -1, 2, -2, 3, -3, 4)]
+    value, gate = project([(z, mix_all) for z in nearest], col_now, arrive_now)
+    near_recv[me_y, :, :feats] = value.astype(BF16)
+    near_recv[me_y, :, feats:] = gate.astype(BF16)
+    for j in ROW_FAR_FIRST:
+        if j:
+            near_copy(partner(me_y, j, per)).start()
     update(0, u_keep[...])
     total, mixer = prepare(1)
-    swap_send[:rows_d] = jnp.concatenate([total, total], axis=1)
-    swap_send[rows_d:] = jnp.concatenate([mixer, mixer], axis=1)
+    tight = mixer[:, :chans]
+    for g in range(1, groups):
+        tight = tight + mixer[:, g * chans : (g + 1) * chans]
+    blank = jnp.zeros((rows_d, width - width // rows_d * chans), F32)
+    swap_send[...] = jnp.concatenate(
+        [total] + [tight[i : i + rows_d] for i in range(0, width, rows_d)] + [blank], axis=1
+    )
 
     @pl.when(me_z != me_d)
     def _():
@@ -328,92 +350,101 @@
     def _():
         swap_recv[...] = swap_send[...]
 
-    for k in reversed(PLANE_FAR_FIRST[:6]):
-        gather_near(k)
     col_wait(1, 1)
     col_start(1, 2)
+
     @pl.when(me_z != me_d)
     def _():
         sent(x_all, x_ss)
+        sent(mix_all, mix_ss)
 
     @pl.when(me_z == me_d)
     def _():
         sent(x_all.at[pl.ds(0, tp - 1)], x_ss)
+        sent(mix_all.at[pl.ds(0, dp - 1)], mix_ss)
 
     sent(near_in.at[pl.ds(0, dp - 1)], in_ss)
-    sent(mix_all.at[pl.ds(0, dp - 1)], mix_ss)
     sent(gain_all.at[pl.ds(0, dp - 1)], gain_ss)
-    sent(col_in.at[pl.ds(0, 7)], col_ss.at[0])
+    sent(x_old.at[pl.ds(0, per - 1)], old_ss)
+    sent(col_now.at[pl.ds(0, 7), 0], col_ss.at[2])
+    sent(col_now.at[pl.ds(0, 7), 1], col_ss.at[3])
+    arrival(x_old.at[pl.ds(0, per - 1)], old_rs).wait_recv()
+    arrival(near_recv.at[pl.ds(0, per - 1)], near_rs).wait_recv()
+    combined = near_recv[0].astype(F32)
+    for y in range(1, per):
+        combined = combined + near_recv[y].astype(F32)
+    fresh = (
+        x_old[...].astype(F32).reshape(rows_d, feats) + combined[:, :feats] * jax.nn.sigmoid(combined[:, feats:])
+    ).astype(BF16)
+
+    x_keep[...] = fresh.reshape(per, rows_t, feats)
+    x = fresh.astype(F32)
+    normed = (x * gain_ref[1:2, :]).astype(BF16)
+    squares = jnp.sum(x * x, axis=1, keepdims=True)
+    upper = squares.astype(BF16).astype(F32)
+    middle = (squares - upper).astype(BF16).astype(F32)
+    lower = squares - upper - middle
+    tail_lane = lax.broadcasted_iota(jnp.int32, (rows_d, 128 - width), 1)
+    tail = jnp.where(tail_lane == 0, upper, jnp.where(tail_lane == 1, middle, jnp.where(tail_lane == 2, lower, 0.0)))
     col_wait(0, 3)
-    for k in reversed(range(1, dp)):
-        row_copy(partner(me_d, k, dp)).start()
-    combined = comb_own[...]
-    arrival(comb_recv.at[pl.ds(0, dp - 1)], comb_rs).wait_recv()
-    for k in range(1, dp):
-        combined = combined + comb_recv[partner(me_z, k, dp)].astype(F32)
-    fresh = (stream_ref[...].astype(F32) + combined[:, :feats] * jax.nn.sigmoid(combined[:, feats:])).astype(BF16)
-
-    x_far[me_d * per + me_y] = fresh
+    own = None
     for k in PLANE_FAR_FIRST:
-        for j in ROW_FAR_FIRST:
-            if k or j:
-                xf_copy(partner(me_y, j, per), partner(me_d, k, dp)).start()
+        to = partner(me_d, k, dp)
+        product = lax.dot_general(normed, col_in[to], NT, preferred_element_type=F32)
+        whole = jnp.concatenate([product, tail], axis=1)
+        if k:
+            part_send[to] = whole.astype(BF16)
+            part_copy(to).start()
+        else:
+            own = whole
     col_wait(1, 2)
     col_start(1, 3, 4)
-    sent(comb_send.at[pl.ds(0, dp - 1)], comb_ss)
-    sent(near_send.at[:, pl.ds(0, per - 1)], near_ss)
+    sent(near_recv.at[pl.ds(0, per - 1)], near_ss)
+    sent(col_in.at[pl.ds(0, 7)], col_ss.at[0])
 
     @pl.when(me_z != me_d)
     def _():
         swap_copy().wait_send()
-
-    acc = jnp.zeros((rows_d, width), F32)
-    squares = jnp.zeros((rows_d, feats), F32)
-    for k in reversed(PLANE_FAR_FIRST):
-        by = partner(me_d, k, dp, True)
-        arrival(x_far.at[pl.ds(0, per if k else per - 1)], xf_rs.at[by]).wait_recv()
-        if k == 1:
-            arrival(far_in.at[pl.ds(0, dp - 1)], row_rs).wait_recv()
-        weights = far_in.at[by] if k else col_in.at[me_d]
-        x = x_far[pl.ds(by * per, per)].astype(F32)
-        normed = (x * gain_all[by, 1][None]).astype(BF16).reshape(rows_d, feats)
-        x = x.reshape(rows_d, feats)
-        squares = squares + x * x
-        acc = acc + lax.dot_general(normed, weights[...], NT, preferred_element_type=F32)
-    u = lax.rsqrt(jnp.sum(squares, axis=1, keepdims=True) / (feats * dp) + EPS) * acc
+        arrival(swap_recv, swap_rs).wait_recv()
+
+    swapped = swap_recv[...]
+    tight = jnp.concatenate(
+        [swapped[:, width + i * chans : width + (i + 1) * chans] for i in range(width // rows_d)], axis=0
+    )
+    mixer = jnp.where(wide_0 // chans == wide_1 // chans, jnp.concatenate([tight] * groups, axis=1), 0.0)
+    arrival(part_recv.at[pl.ds(0, dp - 1)], part_rs).wait_recv()
+    for k in range(1, dp):
+        own = own + part_recv[partner(me_d, k, dp)].astype(F32)
+    squares = own[:, width : width + 1] + own[:, width + 1 : width + 2] + own[:, width + 2 : width + 3]
+    u = lax.rsqrt(squares / (feats * dp) + EPS) * own[:, :width]
     u_send[...] = jnp.concatenate([u, u], axis=1)
 
     @pl.when(me_z != me_d)
     def _():
         u_copy().start()
-        arrival(swap_recv, swap_rs).wait_recv()
 
     @pl.when(me_z == me_d)
     def _():
         u_recv[...] = u_send[...]
 
-    pre = swap_recv[:rows_d, :width] + jnp.dot(
-        u, swap_recv[rows_d:, :width], precision=HIGHEST, preferred_element_type=F32
-    )
-    mix_far[me_d] = jax.nn.gelu(pre).astype(BF16)
+    pre = swapped[:, :width] + jnp.dot(u, mixer, precision=HIGHEST, preferred_element_type=F32)
+    mix_far[me_d] = fold(jax.nn.gelu(pre).astype(BF16))
     for k in PLANE_FAR_FIRST:
         if k:
             mf_copy(partner(me_d, k, dp)).start()
     col_wait(1, 3)
-    sent(x_far.at[pl.ds(0, tp - 1)], xf_ss)
-    sent(far_in.at[pl.ds(0, dp - 1)], row_ss)
+    sent(part_send.at[pl.ds(0, dp - 1)], part_ss)
     sent(col_out.at[pl.ds(0, 7)], col_ss.at[1])
-    value = jnp.zeros((rows_d, feats), F32)
-    gate = jnp.zeros((rows_d, feats), F32)
-    for k in reversed(PLANE_FAR_FIRST):
-        by = partner(me_d, k, dp, True)
-        if k:
-            arrival(mix_far.at[by], mix_rs.at[by]).wait_recv()
-        mixed = mix_far[by]
-        value = value + jnp.dot(mixed, col_out[by, 0], preferred_element_type=F32)
-        gate = gate + jnp.dot(mixed, col_out[by, 1], preferred_element_type=F32)
-    near_own[0, :, :, :feats] = value.reshape(per, rows_t, feats)
-    near_own[0, :, :, feats:] = gate.reshape(per, rows_t, feats)
+
+    def arrive_far(i, block):
+        if i:
+            arrival(mix_far.at[block], mix_rs.at[block]).wait_recv()
+
+    value, gate = project(
+        [(partner(me_d, k, dp, True), mix_far) for k in reversed(PLANE_FAR_FIRST)], col_out, arrive_far
+    )
+    out_own[:, :, :feats] = value.reshape(per, rows_t, feats)
+    out_own[:, :, feats:] = gate.reshape(per, rows_t, feats)
     out_send[:, :, :feats] = value.astype(BF16).reshape(per, rows_t, feats)
     out_send[:, :, feats:] = gate.astype(BF16).reshape(per, rows_t, feats)
     for j in ROW_FAR_FIRST:
@@ -425,12 +456,12 @@
         arrival(u_recv, u_rs).wait_recv()
 
     update(1, u_recv[:, :width])
-    combined = near_own[0, me_y]
+    combined = out_own[me_y]
     arrival(out_recv.at[pl.ds(0, per - 1)], of_rs).wait_recv()
     for j in range(1, per):
         combined = combined + out_recv[partner(me_y, j, per)].astype(F32)
     out_ref[...] = (
-        x_far[me_d * per + me_y].astype(F32) + combined[:, :feats] * jax.nn.sigmoid(combined[:, feats:])
+        x_keep[me_y].astype(F32) + combined[:, :feats] * jax.nn.sigmoid(combined[:, feats:])
     ).astype(BF16)
 
     sent(mix_far.at[pl.ds(0, dp - 1)], mf_ss)
@@ -483,7 +514,7 @@
             pltpu.VMEM(lam_im.shape, F32),
             pltpu.VMEM(log_dt.shape, F32),
             pltpu.VMEM(d_skip.shape, F32),
-            pltpu.VMEM((3, width, feats), BF16),
+            pltpu.VMEM((width, feats), BF16),
             pltpu.VMEM(turned_re.shape, F32),
             pltpu.VMEM(turned_im.shape, F32),
             pltpu.VMEM(readout_real.shape, F32),
@@ -497,36 +528,35 @@
             pltpu.VMEM((rows_d, width), F32),
             pltpu.VMEM((width, width), F32),
             pltpu.VMEM((tp, rows_t, feats), BF16),
+            pltpu.VMEM((per, rows_t, feats), BF16),
             pltpu.VMEM((dp, width, feats), BF16),
-            pltpu.VMEM((dp, rows_d, width), BF16),
-            pltpu.VMEM((dp, per, rows_t, 2 * feats), F32),
-            pltpu.VMEM((dp, per, rows_t, 2 * feats), BF16),
-            pltpu.VMEM((dp, per, rows_t, 2 * feats), BF16),
-            pltpu.VMEM((dp, rows_t, 2 * feats), BF16),
-            pltpu.VMEM((rows_t, 2 * feats), F32),
-            pltpu.VMEM((dp, rows_t, 2 * feats), BF16),
-            pltpu.VMEM((dp, layers, rows_t, feats), F32),
+            pltpu.VMEM((rows_d // 2, 2 * width), BF16),
+            pltpu.VMEM((dp, rows_d // 2, 2 * width), BF16),
+            pltpu.VMEM((per, rows_d, 2 * feats), BF16),
+            pltpu.VMEM((per, rows_t, 2 * feats), F32),
+            pltpu.VMEM((dp, rows_t, feats), F32),
             pltpu.VMEM((dp, width, feats), BF16),
             pltpu.VMEM((dp, 2, width, feats), BF16),
-            pltpu.VMEM((dp, width, feats), BF16),
-            pltpu.VMEM((tp, rows_t, feats), BF16),
-            pltpu.VMEM((rows_d + width, 128), F32),
-            pltpu.VMEM((rows_d + width, 128), F32),
+            pltpu.VMEM((dp, 2, width, feats), BF16),
+            pltpu.VMEM((per, rows_t, feats), BF16),
+            pltpu.VMEM((dp, rows_d, 128), BF16),
+            pltpu.VMEM((dp, rows_d, 128), BF16),
+            pltpu.VMEM((rows_d, 2 * width), F32),
+            pltpu.VMEM((rows_d, 2 * width), F32),
             pltpu.VMEM((rows_d, 128), F32),
             pltpu.VMEM((rows_d, 128), F32),
-            pltpu.VMEM((dp, rows_d, width), BF16),
+            pltpu.VMEM((dp, rows_d // 2, 2 * width), BF16),
             pltpu.VMEM((per, rows_t, 2 * feats), BF16),
             pltpu.VMEM((per, rows_t, 2 * feats), BF16),
             dma(6), dma(11),
             one, dma(dp),
             one, one,
-            one, dma(dp),
+            one, one,
             one, dma(dp),
             one, one,
             one, one,
-            dma(2), dma(2, 3),
+            dma(4), dma(4, 3),
             one, one,
-            one, dma(dp),
             one, one,
             one, one,
             one, one, one,

time: 46.2 us -> 45.1 us (0.976)
  Pallas kernels: 45.5 us -> 44.4 us
    pallas_call x1, Pallas kernels: 44.8 us -> 43.7 us  [per_device(): pl.pallas_call(functools.partial(kernel, tp, dp, chans), out_shape=(pltpu...]
where the time goes in v7:
time: 45.1 us; the launch traced here: 45 us
  Pallas kernels  44.4 us (98%)
  between operations  0.64 us (1%)
    pallas_call x1, Pallas kernels, per_device(): pl.pallas_call(functools.partial(kernel, tp, dp, chans), out_shape=(pltpu...  43.7 us

profile of v7, /device:TPU:1, one launch (start us, length us, event | category | flops | bytes accessed | tf_op | source)
XLA Modules:
  0.0 45.0 jit_solution(3745168018617468630)
XLA Ops:
  0.6 43.7 %shard_map.149 = (bf16[8,256]{1,0:T(8,128)(2,1)S(1)}, f32[2,128,128]{2,1,0:T(8,128)S(1)}) custom-call(bf16[8,256]{1,0:T(8,128)(2,1)} %stream_hbm.1, f32[2,256]{1,0:T(2,128)} %gain_hbm.1, bf16[2,64,256]{2,1,0:T(8,128)(2,1)} %bitcast.6, f32[2,4,64]{2,1,0:T(4,128)} %lam_re_hbm.1, f32[2,4,64]{2,1,0:T(4,128)} %lam_im_hbm.1, f32[2,4]{1,0:T(2,128)} %log_dt_hbm.1, ...), custom_call_target="tpu_custom_call" | custom-call | tf_op jit(solution)/shard_map/pallas_call | solution.py:505
  44.3 0.7 %shard_map.150 = (bf16[8,256]{1,0:T(8,128)(2,1)}, f32[2,128,128]{2,1,0:T(8,128)}) custom-call(bf16[8,256]{1,0:T(8,128)(2,1)S(1)} %get-tuple-element.6.out_ref, f32[2,128,128]{2,1,0:T(8,128)S(1)} %get-tuple-element.7.states_ref), custom_call_target="tpu_custom_call" | custom-call | tf_op jit(solution)/shard_map/pallas_call | solution.py:570

commit v8 on v7

--- a/solution.py
+++ b/solution.py
@@ -118,10 +118,7 @@
 
     def col_part(what, home, side, i):
         rows = pl.ds(side * (width // 2), width // 2)
-        if what == 1:
-            held = col_out.at[home]
-            return held.at[:, rows] if i == 4 else held
-        held = col_now.at[home, what - 2] if what else col_in.at[home]
+        held = (col_in.at[home], col_out.at[home, 0], col_now.at[home, 0], col_now.at[home, 1], col_out.at[home, 1])[what]
         return held.at[rows] if i == 4 else held
 
     def col_copy(what, side, i):
@@ -138,7 +135,9 @@
 
     def col_wait(what, hop):
         blocks = pl.ds(0, 3 if hop == 3 else 2)
-        held = (col_in.at[blocks], col_out.at[blocks], col_now.at[blocks, 0], col_now.at[blocks, 1])[what]
+        held = (
+            col_in.at[blocks], col_out.at[blocks, 0], col_now.at[blocks, 0], col_now.at[blocks, 1], col_out.at[blocks, 1]
+        )[what]
         arrival(held, col_rs.at[what, hop - 1]).wait_recv()
 
     def part_copy(to):
@@ -293,12 +292,13 @@
 
     for what in (2, 3):
         col_wait(what, 2)
-        col_start(what, 3, 4)
+        col_start(what, 4, 3)
     col_wait(0, 1)
     col_start(0, 2)
     loads[9].wait()
     loads[10].wait()
     col_start(1, 1)
+    col_start(4, 1)
 
     def project(blocks, weights, arrive):
         value = jnp.zeros((rows_d, feats), F32)
@@ -316,7 +316,7 @@
             col_wait(2, 3)
             col_wait(3, 3)
             col_wait(0, 2)
-            col_start(0, 3, 4)
+            col_start(0, 4, 3)
         if i:
             arrival(mix_all.at[block], mix_rs.at[block]).wait_recv()
         else:
@@ -350,8 +350,9 @@
     def _():
         swap_recv[...] = swap_send[...]
 
-    col_wait(1, 1)
-    col_start(1, 2)
+    for what in (1, 4):
+        col_wait(what, 1)
+        col_start(what, 2)
 
     @pl.when(me_z != me_d)
     def _():
@@ -397,8 +398,9 @@
             part_copy(to).start()
         else:
             own = whole
-    col_wait(1, 2)
-    col_start(1, 3, 4)
+    for what in (1, 4):
+        col_wait(what, 2)
+        col_start(what, 4, 3)
     sent(near_recv.at[pl.ds(0, per - 1)], near_ss)
     sent(col_in.at[pl.ds(0, 7)], col_ss.at[0])
 
@@ -433,8 +435,10 @@
         if k:
             mf_copy(partner(me_d, k, dp)).start()
     col_wait(1, 3)
+    col_wait(4, 3)
     sent(part_send.at[pl.ds(0, dp - 1)], part_ss)
-    sent(col_out.at[pl.ds(0, 7)], col_ss.at[1])
+    sent(col_out.at[pl.ds(0, 7), 0], col_ss.at[1])
+    sent(col_out.at[pl.ds(0, 7), 1], col_ss.at[4])
 
     def arrive_far(i, block):
         if i:
@@ -555,7 +559,7 @@
             one, dma(dp),
             one, one,
             one, one,
-            dma(4), dma(4, 3),
+            dma(5), dma(5, 3),
             one, one,
             one, one,
             one, one,

time: 45.1 us -> 45.2 us (level)
  no operation moved by 1% of the time
where the time goes in v8:
time: 45.2 us; the launch traced here: 45.1 us
  Pallas kernels  44.5 us (98%)
  between operations  0.64 us (1%)
    pallas_call x1, Pallas kernels, per_device(): pl.pallas_call(functools.partial(kernel, tp, dp, chans), out_shape=(pltpu...  43.8 us

profile of v8, /device:TPU:1, one launch (start us, length us, event | category | flops | bytes accessed | tf_op | source)
XLA Modules:
  0.0 45.1 jit_solution(10980267478424491623)
XLA Ops:
  0.6 43.8 %shard_map.149 = (bf16[8,256]{1,0:T(8,128)(2,1)S(1)}, f32[2,128,128]{2,1,0:T(8,128)S(1)}) custom-call(bf16[8,256]{1,0:T(8,128)(2,1)} %stream_hbm.1, f32[2,256]{1,0:T(2,128)} %gain_hbm.1, bf16[2,64,256]{2,1,0:T(8,128)(2,1)} %bitcast.6, f32[2,4,64]{2,1,0:T(4,128)} %lam_re_hbm.1, f32[2,4,64]{2,1,0:T(4,128)} %lam_im_hbm.1, f32[2,4]{1,0:T(2,128)} %log_dt_hbm.1, ...), custom_call_target="tpu_custom_call" | custom-call | tf_op jit(solution)/shard_map/pallas_call | solution.py:509
  44.5 0.7 %shard_map.150 = (bf16[8,256]{1,0:T(8,128)(2,1)}, f32[2,128,128]{2,1,0:T(8,128)}) custom-call(bf16[8,256]{1,0:T(8,128)(2,1)S(1)} %get-tuple-element.6.out_ref, f32[2,128,128]{2,1,0:T(8,128)S(1)} %get-tuple-element.7.states_ref), custom_call_target="tpu_custom_call" | custom-call | tf_op jit(solution)/shard_map/pallas_call | solution.py:574

commit v9 on v8

--- a/solution.py
+++ b/solution.py
@@ -116,17 +116,24 @@
     def gain_copy(to):
         return send(gain_all.at[me_d], gain_all.at[me_d], gain_ss, gain_rs, me_t, to)
 
+    now = (3, 4, 5, 6)
+
+    def col_stream(what, home):
+        if what < 3:
+            return (col_in.at[home], col_out.at[home, 0], col_out.at[home, 1])[what]
+        return col_now.at[home, (what - 3) // 2, pl.ds((what - 3) % 2 * (width // 2), width // 2)]
+
     def col_part(what, home, side, i):
-        rows = pl.ds(side * (width // 2), width // 2)
-        held = (col_in.at[home], col_out.at[home, 0], col_now.at[home, 0], col_now.at[home, 1], col_out.at[home, 1])[what]
-        return held.at[rows] if i == 4 else held
+        held = col_stream(what, home)
+        rows = held.shape[0] // 2
+        return held.at[pl.ds(side * rows, rows)] if i == 4 else held
 
     def col_copy(what, side, i):
         sign = 1 - 2 * side
         home = lax.rem(me_z - sign * min(i - 1, 2) + 2 * dp, dp)
         to = lax.rem(me_z + sign * (2 if i == 4 else 1) + dp, dp)
         part = col_part(what, home, side, i)
-        return send(part, part, col_ss.at[what], col_rs.at[what, min(i, 3) - 1], to * per + me_y, me_d)
+        return send(part, part, col_ss.at[(0, 1, 1, 2, 2, 2, 2)[what]], col_rs.at[what, min(i, 3) - 1], to * per + me_y, me_d)
 
     def col_start(what, *hops):
         for i in hops:
@@ -135,9 +142,7 @@
 
     def col_wait(what, hop):
         blocks = pl.ds(0, 3 if hop == 3 else 2)
-        held = (
-            col_in.at[blocks], col_out.at[blocks, 0], col_now.at[blocks, 0], col_now.at[blocks, 1], col_out.at[blocks, 1]
-        )[what]
+        held = col_stream(what, blocks)
         arrival(held, col_rs.at[what, hop - 1]).wait_recv()
 
     def part_copy(to):
@@ -239,13 +244,13 @@
             old_copy(partner(me_y, j, per)).start()
     loads[7].wait()
     loads[8].wait()
-    col_start(2, 1)
-    col_start(3, 1)
+    for what in now:
+        col_start(what, 1)
     for small in smalls[2:]:
         small.wait()
     from_old[...], mix_w[...] = prepare(0)
 
-    for what in (2, 3):
+    for what in now:
         col_wait(what, 1)
         col_start(what, 2)
     loads[1].wait()
@@ -290,7 +295,7 @@
     def _():
         mix_all[me_z] = mix_out[...]
 
-    for what in (2, 3):
+    for what in now:
         col_wait(what, 2)
         col_start(what, 4, 3)
     col_wait(0, 1)
@@ -298,7 +303,7 @@
     loads[9].wait()
     loads[10].wait()
     col_start(1, 1)
-    col_start(4, 1)
+    col_start(2, 1)
 
     def project(blocks, weights, arrive):
         value = jnp.zeros((rows_d, feats), F32)
@@ -313,8 +318,8 @@
 
     def arrive_now(i, block):
         if i == 5:
-            col_wait(2, 3)
-            col_wait(3, 3)
+            for what in now:
+                col_wait(what, 3)
             col_wait(0, 2)
             col_start(0, 4, 3)
         if i:
@@ -350,7 +355,7 @@
     def _():
         swap_recv[...] = swap_send[...]
 
-    for what in (1, 4):
+    for what in (1, 2):
         col_wait(what, 1)
         col_start(what, 2)
 
@@ -367,8 +372,7 @@
     sent(near_in.at[pl.ds(0, dp - 1)], in_ss)
     sent(gain_all.at[pl.ds(0, dp - 1)], gain_ss)
     sent(x_old.at[pl.ds(0, per - 1)], old_ss)
-    sent(col_now.at[pl.ds(0, 7), 0], col_ss.at[2])
-    sent(col_now.at[pl.ds(0, 7), 1], col_ss.at[3])
+    sent(col_now.at[pl.ds(0, 7)], col_ss.at[2])
     arrival(x_old.at[pl.ds(0, per - 1)], old_rs).wait_recv()
     arrival(near_recv.at[pl.ds(0, per - 1)], near_rs).wait_recv()
     combined = near_recv[0].astype(F32)
@@ -398,7 +402,7 @@
             part_copy(to).start()
         else:
             own = whole
-    for what in (1, 4):
+    for what in (1, 2):
         col_wait(what, 2)
         col_start(what, 4, 3)
     sent(near_recv.at[pl.ds(0, per - 1)], near_ss)
@@ -435,10 +439,9 @@
         if k:
             mf_copy(partner(me_d, k, dp)).start()
     col_wait(1, 3)
-    col_wait(4, 3)
+    col_wait(2, 3)
     sent(part_send.at[pl.ds(0, dp - 1)], part_ss)
-    sent(col_out.at[pl.ds(0, 7), 0], col_ss.at[1])
-    sent(col_out.at[pl.ds(0, 7), 1], col_ss.at[4])
+    sent(col_out.at[pl.ds(0, 7)], col_ss.at[1])
 
     def arrive_far(i, block):
         if i:
@@ -559,7 +562,7 @@
             one, dma(dp),
             one, one,
             one, one,
-            dma(5), dma(5, 3),
+            dma(3), dma(7, 3),
             one, one,
             one, one,
             one, one,

time: 45.2 us -> 45.1 us (level)
  no operation moved by 1% of the time
where the time goes in v9:
time: 45.1 us; the launch traced here: 45 us
  Pallas kernels  44.4 us (98%)
  between operations  0.64 us (1%)
    pallas_call x1, Pallas kernels, per_device(): pl.pallas_call(functools.partial(kernel, tp, dp, chans), out_shape=(pltpu...  43.7 us

profile of v9, /device:TPU:1, one launch (start us, length us, event | category | flops | bytes accessed | tf_op | source)
XLA Modules:
  0.0 45.0 jit_solution(7137139873337290392)
XLA Ops:
  0.6 43.7 %shard_map.149 = (bf16[8,256]{1,0:T(8,128)(2,1)S(1)}, f32[2,128,128]{2,1,0:T(8,128)S(1)}) custom-call(bf16[8,256]{1,0:T(8,128)(2,1)} %stream_hbm.1, f32[2,256]{1,0:T(2,128)} %gain_hbm.1, bf16[2,64,256]{2,1,0:T(8,128)(2,1)} %bitcast.6, f32[2,4,64]{2,1,0:T(4,128)} %lam_re_hbm.1, f32[2,4,64]{2,1,0:T(4,128)} %lam_im_hbm.1, f32[2,4]{1,0:T(2,128)} %log_dt_hbm.1, ...), custom_call_target="tpu_custom_call" | custom-call | tf_op jit(solution)/shard_map/pallas_call | solution.py:512
  44.4 0.7 %shard_map.150 = (bf16[8,256]{1,0:T(8,128)(2,1)}, f32[2,128,128]{2,1,0:T(8,128)}) custom-call(bf16[8,256]{1,0:T(8,128)(2,1)S(1)} %get-tuple-element.6.out_ref, f32[2,128,128]{2,1,0:T(8,128)S(1)} %get-tuple-element.7.states_ref), custom_call_target="tpu_custom_call" | custom-call | tf_op jit(solution)/shard_map/pallas_call | solution.py:577
